TPU v7x, 32 devices: a whole 2x2x4 slice. The times are simulated.
32 devices in a mesh: dp: 4 (over y, x), kv: 4 (over z), tp: 2 (over core).
Axes of the slice: x: 2, y: 2, z: 4, core: 2. Of those that a mesh axis runs over, the one named last changes fastest.
Arguments:
- tokens: bfloat16 [4, 3072, 2048], P('dp', 'kv'), may hold values from -60 to 60
- query_weight: bfloat16 [2048, 1024], P(None, 'tp'), may hold values from -0.125 to 0.125
- key_weight: bfloat16 [2048, 256], P(None, 'tp'), may hold values from -0.125 to 0.125
- value_weight: bfloat16 [2048, 256], P(None, 'tp'), may hold values from -0.125 to 0.125
- out_weight: bfloat16 [1024, 2048], P('tp'), may hold values from -3 to 3
- norm_gain: float32 [2048], P('tp'), may hold values from 0.1 to 1.9
- chosen_owner: int32 [4, 24, 4], P('dp'), may hold values from -1 to 3, as said below
- chosen_part: int32 [4, 24, 4], P('dp'), may hold values from 0 to 11, as said below
Outputs:
- attended: bfloat16 [4, 3072, 2048], P('dp', 'kv', 'tp')
Inputs may be any that keep to these rules, and one draw needn't show every extreme that they name: `chosen_owner`: within a row the indices other than -1 are different. Every named key block lies wholly before its query block's first position. Among the 6 rows of one index of kv, no index is named by more than 6 rows. `chosen_part`: 0 where the owner is -1.
All inputs are finite; a program needn't handle non-finite values.
Results may differ from a plain program's by a relative error of at most 0.014.
The roundings to bfloat16 on the way count: a program that leaves them out, or rounds other values in their place, can miss the bound.
Values may be sent and summed in bfloat16 or wider, within the bound.
No kernel may reach another device: no remote copies, remote signals or barrier semaphores. Data moves between devices by JAX's collectives and lax.ppermute only.
A program may use at most 128 MiB of HBM per device.

v0:
```python
import jax
import jax.numpy as jnp
from jax import lax
from jax.sharding import PartitionSpec as P

D = 2048
HEAD_DIM = 64
QUERY_BLOCK = 128
KEY_BLOCK = 64


rope_base = 10000.0
norm_eps = 1e-06


def rotate(head_rows, positions):
    half_dim = head_rows.shape[-1] // 2
    frequency = rope_base ** (-jnp.arange(half_dim, dtype=jnp.float32) / half_dim)
    angles = positions.astype(jnp.float32)[:, None] * frequency
    cosine = jnp.cos(angles)[:, None, :]
    sine_part = jnp.sin(angles)[:, None, :]
    first_half = head_rows[..., :half_dim]
    second_half = head_rows[..., half_dim:]
    return jnp.concatenate(
        [
            first_half * cosine - second_half * sine_part,
            second_half * cosine + first_half * sine_part,
        ],
        axis=-1,
    )


def rank_within(flat_ids):
    entry_count = flat_ids.shape[0]
    same_owner = flat_ids[:, None] == flat_ids[None, :]
    earlier = jnp.arange(entry_count)[None, :] < jnp.arange(entry_count)[:, None]
    return jnp.sum(jnp.logical_and(same_owner, earlier), axis=1)


def body(
    tokens, query_weight, key_weight, value_weight, out_weight, norm_gain, chosen_owner, chosen_part
):
    row_data = tokens[0]
    tok_count = row_data.shape[0]
    devices = lax.axis_size("kv")
    my_index = lax.axis_index("kv")
    positions = my_index * tok_count + jnp.arange(tok_count, dtype=jnp.int32)
    heads_here = query_weight.shape[1] // HEAD_DIM
    kv_here = key_weight.shape[1] // HEAD_DIM
    group_size = heads_here // kv_here
    kv_width = kv_here * HEAD_DIM
    queries = rotate(
        jnp.dot(row_data, query_weight, preferred_element_type=jnp.float32).reshape(
            tok_count, heads_here, HEAD_DIM
        ),
        positions,
    ).astype(jnp.bfloat16)
    key_rows = (
        rotate(
            jnp.dot(row_data, key_weight, preferred_element_type=jnp.float32).reshape(
                tok_count, kv_here, HEAD_DIM
            ),
            positions,
        )
        .astype(jnp.bfloat16)
        .reshape(tok_count, kv_width)
    )
    value_rows = jnp.dot(row_data, value_weight, preferred_element_type=jnp.float32).astype(
        jnp.bfloat16
    )
    per_device = tok_count // KEY_BLOCK
    qblocks = tok_count // QUERY_BLOCK
    chosen_count = chosen_owner.shape[2]
    owner_ids = chosen_owner[0]
    part_ids = chosen_part[0]
    mine_owner = lax.dynamic_slice_in_dim(owner_ids, my_index * qblocks, qblocks, 0).reshape(
        qblocks * chosen_count
    )
    mine_valid = mine_owner >= 0
    key_blocks = key_rows.reshape(per_device, KEY_BLOCK, kv_width)
    value_blocks = value_rows.reshape(per_device, KEY_BLOCK, kv_width)
    every_owner = owner_ids.reshape(devices, qblocks * chosen_count)
    every_part = part_ids.reshape(devices, qblocks * chosen_count)
    every_rank = jax.vmap(rank_within)(every_owner)
    slot_ids = jnp.arange(qblocks, dtype=jnp.int32)
    picked_mask = jnp.logical_and(
        (every_owner == my_index)[:, None, :], every_rank[:, None, :] == slot_ids[None, :, None]
    )
    wanted = jnp.sum(jnp.where(picked_mask, every_part[:, None, :], 0), axis=2)
    send_keys = key_blocks[wanted]
    send_values = value_blocks[wanted]
    got_keys, got_values = (
        lax.all_to_all(send_keys, "kv", split_axis=0, concat_axis=0, tiled=True),
        lax.all_to_all(send_values, "kv", split_axis=0, concat_axis=0, tiled=True),
    )
    slot_index = jnp.where(mine_valid, mine_owner * qblocks + rank_within(mine_owner), 0)
    picked_keys = got_keys.reshape(devices * qblocks, KEY_BLOCK, kv_width)[slot_index]
    picked_values = got_values.reshape(devices * qblocks, KEY_BLOCK, kv_width)[slot_index]
    block_queries = queries.reshape(qblocks, QUERY_BLOCK, kv_here, group_size, HEAD_DIM)
    chosen_keys = picked_keys.reshape(qblocks, chosen_count * KEY_BLOCK, kv_here, HEAD_DIM)
    chosen_values = picked_values.reshape(qblocks, chosen_count * KEY_BLOCK, kv_here, HEAD_DIM)
    all_keys = jnp.concatenate(
        [chosen_keys, key_rows.reshape(qblocks, QUERY_BLOCK, kv_here, HEAD_DIM)], axis=1
    )
    all_values = jnp.concatenate(
        [chosen_values, value_rows.reshape(qblocks, QUERY_BLOCK, kv_here, HEAD_DIM)], axis=1
    )
    key_valid = jnp.broadcast_to(
        mine_valid.reshape(qblocks, chosen_count, 1), (qblocks, chosen_count, KEY_BLOCK)
    ).reshape(qblocks, chosen_count * KEY_BLOCK)
    far_mask = jnp.broadcast_to(
        key_valid[:, None, :], (qblocks, QUERY_BLOCK, chosen_count * KEY_BLOCK)
    )
    lower_mask = jnp.broadcast_to(
        (jnp.arange(QUERY_BLOCK)[:, None] >= jnp.arange(QUERY_BLOCK)[None, :])[None],
        (qblocks, QUERY_BLOCK, QUERY_BLOCK),
    )
    full_mask = jnp.concatenate([far_mask, lower_mask], axis=2)
    scores = jnp.einsum(
        "bqngd,bknd->bngqk", block_queries, all_keys, preferred_element_type=jnp.float32
    ) * HEAD_DIM ** (-0.5)
    scores = jnp.where(full_mask[:, None, None], scores, -jnp.inf)
    row_max = jnp.max(scores, axis=-1, keepdims=True)
    weights = jnp.exp(scores - row_max)
    weights = (weights / jnp.sum(weights, axis=-1, keepdims=True)).astype(jnp.bfloat16)
    mixed_rows = (
        jnp.einsum("bngqk,bknd->bqngd", weights, all_values, preferred_element_type=jnp.float32)
        .astype(jnp.bfloat16)
        .reshape(tok_count, heads_here * HEAD_DIM)
    )
    terms = jnp.dot(mixed_rows, out_weight, preferred_element_type=jnp.float32)
    projected = lax.psum_scatter(
        terms.astype(jnp.bfloat16), "tp", scatter_dimension=1, tiled=True
    ).astype(jnp.float32)
    row_total = lax.psum(jnp.sum(projected * projected, axis=1), "tp")
    scale_rows = lax.rsqrt(row_total / D + norm_eps)
    result = (projected * scale_rows[:, None] * norm_gain[None, :]).astype(jnp.bfloat16)
    return result[None]


def solution(mesh):
    placed = (
        P("dp", "kv", None),
        P(None, "tp"),
        P(None, "tp"),
        P(None, "tp"),
        P("tp", None),
        P("tp"),
        P("dp", None, None),
        P("dp", None, None),
    )
    return jax.shard_map(
        body, mesh=mesh, in_specs=placed, out_specs=P("dp", "kv", "tp"), check_vma=False
    )
```

profile of v0, /device:TPU:31, one launch (start us, length us, event | category | flops | bytes accessed | tf_op | source)
XLA Modules:
  0.0 116.0 jit_solution(5359210719336470150)
XLA Ops:
  6.5 0.6 iota_compare_fusion.2
  7.2 2.3 %copy.52 = bf16[2048,128]{0,1:T(8,128)(2,1)} copy(bf16[2048,128]{1,0:T(8,128)(2,1)} %param.10) | data formatting | bytes 1048576 | tf_op args[2]
  9.5 0.4 multiply_cosine_fusion
  9.9 2.2 %fusion.13 = f32[768,2,64]{0,2,1:T(8,128)S(1)} fusion(bf16[2,64,2048]{2,1,0:T(8,128)(2,1)} %bitcast.97, bf16[1,768,2048]{2,1,0:T(8,128)(2,1)S(1)} %copy-done), kind=kOutput, calls=%fused_computation.22 | convolution fusion | flops 402653184 | bytes 4063232 | tf_op jit(solution)/shard_map/dot_general | solution.py:60
  12.3 0.6 copy-done.2
  12.9 1.1 copy.53
  14.0 1.2 %convert_element_type.47 = bf16[12,64,128]{2,1,0:T(8,128)(2,1)S(1)} reshape(bf16[768,2,64]{2,1,0:T(2,128)(2,1)} %copy.53) | data formatting | bytes 393216 | tf_op jit(solution)/shard_map/convert_element_type | solution.py:65
  15.4 0.5 broadcast_compare_fusion.1
  15.9 1.5 %convert_reduce_fusion = s32[4,24]{1,0:T(4,128)} fusion(s32[4,24]{1,0:T(4,128)S(1)} %reshape_squeeze.3, pred[24,24]{1,0:T(8,128)(4,1)} %iota_compare_fusion.2), kind=kLoop, calls=%fused_computation.49 | loop fusion | flops 9120 | bytes 1344 | tf_op jit(solution)/shard_map/vmap()/reduce_sum | solution.py:37
  17.4 0.8 copy.43
  18.3 0.9 select_reduce_fusion
  19.3 1.4 %gather_fusion.2 = bf16[24,64,128]{2,1,0:T(8,128)(2,1)} fusion(bf16[12,64,128]{2,1,0:T(8,128)(2,1)S(1)} %convert_element_type.47, s32[1024]{0:T(1024)S(1)} %pad_clamp_fusion.1), kind=kCustom, calls=%fused_computation.2 | custom fusion | bytes 786528 | tf_op jit(solution)/shard_map/gather | solution.py:90
  20.7 4.5 %all-to-all-start.1 = ((bf16[4,6,64,128]{3,2,1,0:T(8,128)(2,1)}), bf16[4,6,64,128]{3,2,1,0:T(8,128)(2,1)}, u32[]{:S(2)}, u32[]{:S(2)}) async-start(bf16[4,6,64,128]{3,2,1,0:T(8,128)(2,1)} %bitcast.95), calls=%async_computation.1 | async-start | bytes 786432 | tf_op jit(solution)/shard_map/all_to_all | solution.py:93
  25.2 0.8 broadcast_multiply_fusion
  26.3 0.7 ge.38
  27.1 4.0 %copy.57 = bf16[2048,512]{0,1:T(8,128)(2,1)} copy(bf16[2048,512]{1,0:T(8,128)(2,1)} %param.9) | data formatting | bytes 4194304 | tf_op args[1]
  31.1 4.6 %fusion.11 = f32[768,8,64]{0,2,1:T(8,128)} fusion(bf16[8,64,2048]{2,1,0:T(8,128)(2,1)} %bitcast.92, bf16[1,768,2048]{2,1,0:T(8,128)(2,1)S(1)} %copy-done), kind=kOutput, calls=%fused_computation.20 | convolution fusion | flops 1610612736 | bytes 6815744 | tf_op jit(solution)/shard_map/dot_general | solution.py:53
  35.7 1.0 fusion.20
  36.7 1.3 %gather_fusion = bf16[24,64,128]{2,1,0:T(8,128)(2,1)} fusion(bf16[12,64,128]{2,1,0:T(8,128)(2,1)S(1)} %bitcast.93, s32[1024]{0:T(1024)S(1)} %pad_clamp_fusion.1), kind=kCustom, calls=%fused_computation | custom fusion | bytes 786528 | tf_op jit(solution)/shard_map/gather | solution.py:91
  38.0 0.2 convert_reduce_fusion.1
  38.2 0.5 fusion.43
  38.8 2.5 %subtract_convert_fusion = (bf16[768,8,32]{0,2,1:T(8,128)(2,1)}, bf16[768,8,32]{0,2,1:T(8,128)(2,1)}) fusion(f32[768,8,64]{0,2,1:T(8,128)} %fusion.11, f32[768,32]{0,1:T(8,128)S(1)} %get-tuple-element.12, f32[768,32]{0,1:T(8,128)S(1)} %get-tuple-element.11), kind=kLoop, calls=%fused_computation.35 | loop fusion | flops 1572864 | bytes 2555904 | tf_op jit(solution)/shard_map/convert.3
  41.2 4.5 %all-to-all-start = ((bf16[4,6,64,128]{3,2,1,0:T(8,128)(2,1)}), bf16[4,6,64,128]{3,2,1,0:T(8,128)(2,1)}, u32[]{:S(2)}, u32[]{:S(2)}) async-start(bf16[4,6,64,128]{3,2,1,0:T(8,128)(2,1)} %bitcast.94), calls=%async_computation | async-start | bytes 786432 | tf_op jit(solution)/shard_map/all_to_all | solution.py:94
  45.8 0.7 fusion.29
  46.4 0.9 reshape.247
  47.3 0.1 copy.51
  47.6 2.2 %concatenate.37 = bf16[6,128,2,4,32]{1,0,4,3,2:T(8,128)(2,1)} reshape(bf16[768,8,32]{0,2,1:T(8,128)(2,1)} %get-tuple-element.7) | data formatting | bytes 786432 | tf_op jit(solution)/shard_map/concatenate | solution.py:24
  49.9 1.9 %copy.58 = bf16[6,128,2,4,32]{1,4,3,2,0:T(8,128)(2,1)} copy(bf16[6,128,2,4,32]{1,0,4,3,2:T(8,128)(2,1)} %concatenate.37) | data formatting | bytes 786432 | tf_op jit(solution)/shard_map/concatenate | solution.py:24
  51.7 2.2 %concatenate.38 = bf16[6,128,2,4,32]{1,0,4,3,2:T(8,128)(2,1)} reshape(bf16[768,8,32]{0,2,1:T(8,128)(2,1)} %get-tuple-element.8) | data formatting | bytes 786432 | tf_op jit(solution)/shard_map/concatenate | solution.py:24
  54.0 1.9 %copy.59 = bf16[6,128,2,4,32]{1,4,3,2,0:T(8,128)(2,1)} copy(bf16[6,128,2,4,32]{1,0,4,3,2:T(8,128)(2,1)} %concatenate.38) | data formatting | bytes 786432 | tf_op jit(solution)/shard_map/concatenate | solution.py:24
  55.8 0.9 copy.50
  56.8 0.3 broadcast_in_dim.39
  57.1 0.7 pad_add_fusion
  57.9 1.7 %copy_bitcast_fusion = (bf16[6,128,2,32]{1,3,2,0:T(8,128)(2,1)}, bf16[6,128,2,32]{1,3,2,0:T(8,128)(2,1)}) fusion(bf16[768,2,32]{0,2,1:T(8,128)(2,1)} %copy-done.2, bf16[768,2,32]{0,2,1:T(8,128)(2,1)} %copy-done.3), kind=kLoop, calls=%fused_computation.46 | loop fusion | bytes 393216 | tf_op jit(solution)/shard_map/concatenate | solution.py:24
  59.5 1.6 %gather_fusion.3 = bf16[24,64,128]{2,1,0:T(8,128)(2,1)S(1)} fusion(bf16[24,64,128]{2,1,0:T(8,128)(2,1)} %bitcast.14, s32[1024]{0:T(1024)S(1)} %pad_clamp_fusion), kind=kCustom, calls=%fused_computation.3 | custom fusion | bytes 786528 | tf_op jit(solution)/shard_map/gather | solution.py:97
  61.2 1.2 %reshape.208 = bf16[6,256,2,64]{3,2,1,0:T(2,128)(2,1)} reshape(bf16[24,64,128]{2,1,0:T(8,128)(2,1)S(1)} %gather_fusion.3) | data formatting | bytes 786432 | tf_op jit(solution)/shard_map/reshape | solution.py:100
  62.4 2.9 %copy.56 = bf16[6,256,2,64]{1,3,2,0:T(8,128)(2,1)} copy(bf16[6,256,2,64]{3,2,1,0:T(2,128)(2,1)} %reshape.208) | data formatting | bytes 786432 | tf_op jit(solution)/shard_map/reshape | solution.py:100
  65.3 1.6 %gather_fusion.1 = bf16[24,64,128]{2,1,0:T(8,128)(2,1)S(1)} fusion(bf16[24,64,128]{2,1,0:T(8,128)(2,1)} %bitcast.4, s32[1024]{0:T(1024)S(1)} %pad_clamp_fusion), kind=kCustom, calls=%fused_computation.1 | custom fusion | bytes 786528 | tf_op jit(solution)/shard_map/gather | solution.py:98
  66.9 1.2 %reshape.205 = bf16[6,256,2,64]{3,2,1,0:T(2,128)(2,1)} reshape(bf16[24,64,128]{2,1,0:T(8,128)(2,1)S(1)} %gather_fusion.1) | data formatting | bytes 786432 | tf_op jit(solution)/shard_map/reshape | solution.py:101
  68.1 2.2 %copy.49 = bf16[6,256,2,64]{1,3,2,0:T(8,128)(2,1)S(1)} copy(bf16[6,256,2,64]{3,2,1,0:T(2,128)(2,1)} %reshape.205) | data formatting | bytes 786432 | tf_op jit(solution)/shard_map/reshape | solution.py:101
  70.3 8.9 %fusion.38 = (f32[6,2,4,128]{3,2,1,0:T(4,128)}, f32[6,2,4,128,384]{3,4,2,1,0:T(8,128)}) fusion(pred[6,128,384]{1,2,0:T(8,128)(4,1)} %pad_add_fusion, bf16[6,128,2,4,32]{1,4,3,2,0:T(8,128)(2,1)} %copy.59, bf16[6,128,2,4,32]{1,4,3,2,0:T(8,128)(2,1)} %copy.58, bf16[6,128,2,32]{1,3,2,0:T(8,128)(2,1)} %get-tuple-element.15, ...), kind=kOutput, calls=%fused_computation.74 | convolution fusion | flops 314769792 | bytes 11132928 | tf_op jit(solution)/shard_map/sub | solution.py:124
  79.1 4.8 %fusion.19 = bf16[6,128,2,4,64]{1,4,3,2,0:T(8,128)(2,1)S(1)} fusion(f32[6,2,4,128,384]{3,4,2,1,0:T(8,128)} %get-tuple-element.14, f32[6,2,4,128]{3,2,1,0:T(4,128)} %get-tuple-element.13, bf16[6,128,2,64]{1,3,2,0:T(8,128)(2,1)} %copy.50, bf16[6,256,2,64]{1,3,2,0:T(8,128)(2,1)S(1)} %copy.49), kind=kOutput, calls=%fused_computation.28 | convolution fusion | flops 308281344 | bytes 10838016 | tf_op jit(solution)/shard_map/bngqk,bknd->bqngd/dot_general | solution.py:127
  83.9 0.6 copy.61
  84.5 3.5 %convolution_convert_fusion = bf16[768,2048]{1,0:T(8,128)(2,1)} fusion(bf16[512,2048]{1,0:T(8,128)(2,1)S(1)} %copy-done.7, bf16[64,8,6,128]{3,2,1,0:T(8,128)(2,1)S(1)} %bitcast.96), kind=kOutput, calls=%fused_computation.16 | convolution fusion | flops 1612185600 | bytes 6029312 | tf_op jit(solution)/shard_map/dot_general | solution.py:131
  88.0 13.8 %reduce-scatter.2.cloned.1.call-done = bf16[768,1024]{1,0:T(8,128)(2,1)} async-done(((bf16[768,2048]{1,0:T(8,128)(2,1)}), bf16[768,1024]{1,0:T(8,128)(2,1)}) %reduce-scatter.2.cloned.1.call-update) | async-done | bytes 1572880 | tf_op jit(solution)/shard_map/reduce_scatter | solution.py:132
  101.9 1.8 %fusion.8 = f32[768]{0:T(1024)S(1)} fusion(bf16[768,1024]{1,0:T(8,128)(2,1)} %reduce-scatter.2.cloned.1.call-done), kind=kLoop, calls=%fused_computation.17 | loop fusion | flops 2358528 | bytes 1575936 | tf_op jit(solution)/shard_map/reduce_sum | solution.py:135
  103.7 2.5 %psum.7 = f32[768]{0:T(1024)S(1)} all-reduce(f32[768]{0:T(1024)S(1)} %fusion.8), channel_id=1, replica_groups=mesh['dp'=4,'kv'=4,'tp'=2] {'tp'}, use_global_device_ids=true, to_apply=%region_7.8 | all-reduce | flops 768 | bytes 6144 | tf_op jit(solution)/shard_map/psum | solution.py:135
  106.2 3.0 %fusion.17 = bf16[1,768,1024]{2,1,0:T(8,128)(2,1)} fusion(bf16[768,1024]{1,0:T(8,128)(2,1)} %reduce-scatter.2.cloned.1.call-done, f32[1024]{0:T(1024)S(1)} %copy-done.5, f32[768]{0:T(1024)S(1)} %add_rsqrt_fusion), kind=kLoop, calls=%fused_computation.26 | loop fusion | flops 3145728 | bytes 3152896 | tf_op jit(solution)/shard_map/broadcast_in_dim | solution.py:138
  (44 shorter events, 1.3 us)
Async XLA Ops:
  6.5 3.4 %copy-start = (bf16[1,768,2048]{2,1,0:T(8,128)(2,1)S(1)}, bf16[1,768,2048]{2,1,0:T(8,128)(2,1)}, u32[]{:S(2)}) copy-start(bf16[1,768,2048]{2,1,0:T(8,128)(2,1)} %param.8) | copy-start | bytes 9437188
  9.9 5.3 %copy-start.4 = (s32[1,24,4]{1,2,0:T(4,128)S(1)}, s32[1,24,4]{1,2,0:T(4,128)}, u32[]{:S(2)}) copy-start(s32[1,24,4]{1,2,0:T(4,128)} %param.14) | copy-start | bytes 1156
  12.2 0.6 copy-start.2
  12.2 0.7 copy-start.3
  20.7 20.5 %all-to-all-start.1 = ((bf16[4,6,64,128]{3,2,1,0:T(8,128)(2,1)}), bf16[4,6,64,128]{3,2,1,0:T(8,128)(2,1)}, u32[]{:S(2)}, u32[]{:S(2)}) async-start(bf16[4,6,64,128]{3,2,1,0:T(8,128)(2,1)} %bitcast.95), calls=%async_computation.1 | async-start | bytes 786432 | tf_op jit(solution)/shard_map/all_to_all | solution.py:93
  31.1 4.6 %copy-start.8 = (bf16[2048,128]{1,0:T(8,128)(2,1)S(1)}, bf16[2048,128]{1,0:T(8,128)(2,1)}, u32[]{:S(2)}) copy-start(bf16[2048,128]{1,0:T(8,128)(2,1)} %param.11) | copy-start | bytes 1572868
  38.8 8.6 %copy-start.6 = (pred[6,4]{0,1:T(4,128)(4,1)S(1)}, pred[6,4]{0,1:T(4,128)(4,1)}, u32[]{:S(2)}) copy-start(pred[6,4]{0,1:T(4,128)(4,1)} %fusion.43) | copy-start | bytes 76
  41.2 24.0 %all-to-all-start = ((bf16[4,6,64,128]{3,2,1,0:T(8,128)(2,1)}), bf16[4,6,64,128]{3,2,1,0:T(8,128)(2,1)}, u32[]{:S(2)}, u32[]{:S(2)}) async-start(bf16[4,6,64,128]{3,2,1,0:T(8,128)(2,1)} %bitcast.94), calls=%async_computation | async-start | bytes 786432 | tf_op jit(solution)/shard_map/all_to_all | solution.py:94
  45.7 56.1 %reduce-scatter.2.cloned.1.call-start = ((), (), s32[]{:S(2)}) async-start(), calls=%async_computation.3 | async-start | bytes 4718592 | tf_op jit(solution)/shard_map/reduce_scatter | solution.py:132
  47.3 8.5 %copy-start.1 = (bf16[6,128,2,64]{3,2,1,0:T(2,128)(2,1)S(1)}, bf16[6,128,2,64]{3,2,1,0:T(2,128)(2,1)}, u32[]{:S(2)}) copy-start(bf16[6,128,2,64]{3,2,1,0:T(2,128)(2,1)} %reshape.247) | copy-start | bytes 589828
  79.1 5.4 %copy-start.7 = (bf16[512,2048]{1,0:T(8,128)(2,1)S(1)}, bf16[512,2048]{1,0:T(8,128)(2,1)}, u32[]{:S(2)}) copy-start(bf16[512,2048]{1,0:T(8,128)(2,1)} %param.12) | copy-start | bytes 6291460
  88.0 18.1 %copy-start.5 = (f32[1024]{0:T(1024)S(1)}, f32[1024]{0:T(1024)}, u32[]{:S(2)}) copy-start(f32[1024]{0:T(1024)} %param.13) | copy-start | bytes 12292
Sparse Core Ops, SparseCore 0:
  88.2 13.6 reduce-scatter.1
where the time goes:
time: 118 us; the launch traced here: 116 us
  local copies, waits for them, and re-layouts  37.9 us (32%)
  matrix products  25 us (21%)
  other arithmetic  14.1 us (12%)
  waiting for transfers between devices  13.8 us (12%)
  between operations  13.6 us (12%)
  starting transfers between devices  9.07 us (8%)
  blocking collectives  2.49 us (2%)
    reduce_scatter x1, waiting for transfers between devices, body(): lax.psum_scatter(terms.astype(jnp.bfloat16), 'tp', scatter_dimension=1, t...  13.8 us
    concatenate x6, local copies, waits for them, and re-layouts, rotate(): jnp.concatenate([first_half * cosine - second_half * sine_part, second_ha...  11 us
    sub x1, matrix products, body(): weights = jnp.exp(scores - row_max)  8.85 us
    unnamed x22, local copies, waits for them, and re-layouts  7.87 us
    dot_general x1, matrix products, body(): jnp.einsum('bngqk,bknd->bqngd', weights, all_values, preferred_element_ty...  4.79 us
    dot_general x1, matrix products, body(): jnp.dot(row_data, query_weight, preferred_element_type=jnp.float32)  4.62 us
    all_to_all x1, starting transfers between devices, body(): lax.all_to_all(send_values, 'kv', split_axis=0, concat_axis=0, tiled=True)  4.53 us
    all_to_all x1, starting transfers between devices, body(): lax.all_to_all(send_keys, 'kv', split_axis=0, concat_axis=0, tiled=True)  4.53 us
  transfers between devices with their start and end apart: 3, of which 1 were waited for; matrix products, arithmetic and copies ran while one was open for 31% of the time, Pallas kernels for 0%

commit v1 on v0

v1 whole, which is shorter than its diff:
```python
import functools

import jax
import jax.numpy as jnp
import numpy as np
from jax import lax
from jax.experimental import pallas as pl
from jax.experimental.pallas import tpu as pltpu
from jax.sharding import PartitionSpec as P

HEAD_DIM = 64
QUERY_BLOCK = 128
KEY_BLOCK = 64
LANES = 128
ROPE_BASE = 10000.0
NORM_EPS = 1e-06
LOG2E = 1.4426950408889634
GROUPS = 1

BF16 = jnp.bfloat16
F32 = jnp.float32
HBM = pltpu.MemorySpace.HBM
SMEM = pltpu.MemorySpace.SMEM
VMEM = pltpu.MemorySpace.VMEM


def angle_tables(length):
    half = HEAD_DIM // 2
    frequency = ROPE_BASE ** (-np.arange(half, dtype=np.float64) / half)
    lane_frequency = np.tile(frequency, LANES // half)
    sign = np.tile(np.repeat([-1.0, 1.0], half), LANES // HEAD_DIM)
    coarse = (np.arange(length // KEY_BLOCK) * KEY_BLOCK)[:, None] * lane_frequency
    fine = np.arange(KEY_BLOCK)[:, None] * lane_frequency
    make = lambda a: np.stack([np.cos(a), np.sin(a) * sign], 1).astype(np.float32)
    return make(coarse), np.swapaxes(make(fine), 0, 1).copy()


def rotate_tile(tile, cosine, sine):
    lane = lax.broadcasted_iota(jnp.int32, tile.shape, 1)
    half = HEAD_DIM // 2
    first = (lane % HEAD_DIM) < half
    swapped = jnp.where(
        first, pltpu.roll(tile, LANES - half, 1), pltpu.roll(tile, half, 1)
    )
    return tile * cosine + swapped * sine


def block_angles(coarse_ref, fine_ref, block):
    coarse = coarse_ref[block]
    c_a, s_a = coarse[0:1], coarse[1:2]
    c_b, s_b = fine_ref[0], fine_ref[1]
    return c_a * c_b - s_a * s_b, s_a * c_b + c_a * s_b


def wanted_block(owner_ref, part_ref, row, me):
    total = jnp.int32(0)
    for slot in range(owner_ref.shape[0]):
        total = total + jnp.where(owner_ref[slot, row] == me, part_ref[slot, row], 0)
    return total


def kv_kernel(plan, devices, chunk, *refs):
    (owner_ref, part_ref, tokens_ref, wk_ref, wv_ref, coarse_ref, fine_ref), refs = refs[:7], refs[7:]
    kv_ref, refs = refs[0], refs[1:]
    send_refs, (tok, weight, tok_sem, w_sem) = refs[: len(plan)], refs[len(plan) :]
    rows = tok.shape[0]
    me = lax.axis_index("kv")
    w_copies = [
        pltpu.make_async_copy(src, weight.at[:, pl.ds(at * LANES, LANES)], w_sem.at[at])
        for at, src in enumerate((wk_ref, wv_ref))
    ]
    t_copies = [
        pltpu.make_async_copy(
            tokens_ref.at[0, pl.ds(at * chunk, chunk)], tok.at[pl.ds(at * chunk, chunk)], tok_sem.at[at]
        )
        for at in range(rows // chunk)
    ]
    for copy in w_copies + t_copies:
        copy.start()
    for copy in w_copies:
        copy.wait()
    per_chunk = chunk // KEY_BLOCK
    blocks = rows // KEY_BLOCK
    for at in range(rows // chunk):
        t_copies[at].wait()
        product = jnp.dot(
            tok[pl.ds(at * chunk, chunk)], weight[...], preferred_element_type=F32
        )
        for sub in range(per_chunk):
            block = at * per_chunk + sub
            cosine, sine = block_angles(coarse_ref, fine_ref, me * blocks + block)
            piece = product[sub * KEY_BLOCK : (sub + 1) * KEY_BLOCK]
            kv_ref[block, :, 0:LANES] = rotate_tile(piece[:, :LANES], cosine, sine).astype(BF16)
            kv_ref[block, :, LANES : 2 * LANES] = piece[:, LANES:].astype(BF16)
    qblocks = rows // QUERY_BLOCK
    for (kind, arg, first), out in zip(plan, send_refs):
        if kind == "shift":
            target = jnp.minimum(me + arg, devices - 1)
            for row in range(out.shape[0]):
                out[row] = kv_ref[wanted_block(owner_ref, part_ref, target * qblocks + first + row, me)]
        else:
            def fill(index, carry, out=out):
                out[index] = kv_ref[wanted_block(owner_ref, part_ref, index, me)]
                return carry
            lax.fori_loop(0, out.shape[0], fill, 0)


def q_kernel(tokens_ref, wq_ref, coarse_ref, fine_ref, out_ref):
    rows = tokens_ref.shape[1]
    step = pl.program_id(0)
    total_blocks = pl.num_programs(0) * (rows // KEY_BLOCK)
    me = lax.axis_index("kv")
    product = jnp.dot(tokens_ref[0], wq_ref[...], preferred_element_type=F32) * (HEAD_DIM ** -0.5)
    tiles = product.shape[1] // LANES
    lane = lax.broadcasted_iota(jnp.int32, (KEY_BLOCK, LANES), 1)
    low = lane < HEAD_DIM
    for sub in range(rows // KEY_BLOCK):
        cosine, sine = block_angles(
            coarse_ref, fine_ref, me * total_blocks + step * (rows // KEY_BLOCK) + sub
        )
        span = slice(sub * KEY_BLOCK, (sub + 1) * KEY_BLOCK)
        for tile in range(tiles):
            piece = rotate_tile(product[span, tile * LANES : (tile + 1) * LANES], cosine, sine)
            other = pltpu.roll(piece, HEAD_DIM, 1)
            if tile < tiles // 2:
                even, odd = jnp.where(low, piece, 0.0), jnp.where(low, other, 0.0)
            else:
                even, odd = jnp.where(low, 0.0, other), jnp.where(low, 0.0, piece)
            out_ref[span, (2 * tile) * LANES : (2 * tile + 1) * LANES] = even.astype(BF16)
            out_ref[span, (2 * tile + 1) * LANES : (2 * tile + 2) * LANES] = odd.astype(BF16)


def attention_kernel(sources, valid_ref, q_ref, own_ref, *refs):
    source_refs, out_ref = refs[:sources], refs[sources]
    step = pl.program_id(0)
    heads = q_ref.shape[1] // LANES
    pairs = heads // 2
    own = own_ref[...].reshape(QUERY_BLOCK, 2 * LANES)
    picks = [ref[0] for ref in source_refs]
    keys = jnp.concatenate([p[:, :LANES] for p in picks] + [own[:, :LANES]], axis=0)
    values = jnp.concatenate([p[:, LANES:] for p in picks] + [own[:, LANES:]], axis=0)
    values = jnp.concatenate([values, jnp.ones_like(values)], axis=1)
    far = sources * KEY_BLOCK
    lane = lax.broadcasted_iota(jnp.int32, (1, far), 1)
    bias = jnp.zeros((1, far), F32)
    for at in range(sources):
        level = jnp.where(valid_ref[step, at] > 0, jnp.float32(0), jnp.float32(-jnp.inf))
        bias = jnp.where(lane // KEY_BLOCK == at, level, bias)
    row_id = lax.broadcasted_iota(jnp.int32, (2 * QUERY_BLOCK, QUERY_BLOCK), 0) % QUERY_BLOCK
    col_id = lax.broadcasted_iota(jnp.int32, (2 * QUERY_BLOCK, QUERY_BLOCK), 1)
    lower = row_id >= col_id
    low = lax.broadcasted_iota(jnp.int32, (QUERY_BLOCK, LANES), 1) < HEAD_DIM
    for pair in range(pairs):
        query = jnp.concatenate(
            [q_ref[:, h * LANES : (h + 1) * LANES] for h in (pair, pair + pairs)], axis=0
        )
        scores = lax.dot_general(
            query, keys, (((1,), (1,)), ((), ())), preferred_element_type=F32
        )
        scores = jnp.concatenate(
            [scores[:, :far] + bias, jnp.where(lower, scores[:, far:], -jnp.inf)], axis=1
        )
        row_max = jnp.max(scores, axis=1, keepdims=True)
        weights = jnp.exp2((scores - row_max) * LOG2E).astype(BF16)
        mixed = jnp.dot(weights, values, preferred_element_type=F32)
        top = jnp.where(low, mixed[:QUERY_BLOCK, :LANES], mixed[QUERY_BLOCK:, :LANES])
        bottom = jnp.where(low, mixed[:QUERY_BLOCK, LANES:], mixed[QUERY_BLOCK:, LANES:])
        out_ref[:, pair * LANES : (pair + 1) * LANES] = (top / bottom).astype(BF16)


def out_kernel(mine_ref, other_ref, w_mine_ref, w_other_ref, gain_ref, out_ref, weight, sem):
    cols = out_ref.shape[1]
    depth = w_mine_ref.shape[0]
    heads = depth // HEAD_DIM
    copies = []
    for side, src in enumerate((w_mine_ref, w_other_ref)):
        for slot in range(heads):
            head = slot // 2 + (slot % 2) * (heads // 2)
            copies.append(
                pltpu.make_async_copy(
                    src.at[pl.ds(head * HEAD_DIM, HEAD_DIM)],
                    weight.at[side, pl.ds(slot * HEAD_DIM, HEAD_DIM)],
                    sem.at[side, slot],
                )
            )

    @pl.when(pl.program_id(0) == 0)
    def _():
        for copy in copies:
            copy.start()
        for copy in copies:
            copy.wait()

    mine, other = mine_ref[...], other_ref[...]
    me = lax.axis_index("tp")
    total = None
    width = 512
    kept = []
    for half in range(2):
        for at in range(cols // width):
            start = pl.multiple_of((me if half == 0 else 1 - me) * cols + at * width, width)
            a = jnp.dot(mine, weight[0, :, pl.ds(start, width)], preferred_element_type=F32)
            b = jnp.dot(other, weight[1, :, pl.ds(start, width)], preferred_element_type=F32)
            projected = a.astype(BF16).astype(F32) + b.astype(BF16).astype(F32)
            if half == 0:
                kept.append(projected)
            squares = jnp.sum(projected * projected, axis=1, keepdims=True)
            total = squares if total is None else total + squares
    scale = lax.rsqrt(total / (2 * cols) + NORM_EPS)
    for at, projected in enumerate(kept):
        span = slice(at * width, (at + 1) * width)
        out_ref[:, span] = (projected * scale * gain_ref[:, span]).astype(BF16)


def body(
    tokens, query_weight, key_weight, value_weight, out_weight, norm_gain, chosen_owner, chosen_part
):
    tok_count, width = tokens.shape[1], tokens.shape[2]
    devices = lax.axis_size("kv")
    me = lax.axis_index("kv")
    heads = query_weight.shape[1] // HEAD_DIM
    assert key_weight.shape[1] == LANES and value_weight.shape[1] == LANES
    per_device = tok_count // KEY_BLOCK
    qblocks = tok_count // QUERY_BLOCK
    owner_t, part_t = chosen_owner[0].T, chosen_part[0].T
    chosen = owner_t.shape[0]
    coarse, fine = (jnp.asarray(t) for t in angle_tables(devices * tok_count))
    swap = [(0, 1), (1, 0)]
    vm = pl.BlockSpec(memory_space=VMEM)
    sm = pl.BlockSpec(memory_space=SMEM)
    hb = pl.BlockSpec(memory_space=HBM)

    groups = GROUPS if qblocks % GROUPS == 0 else 1
    per_group = qblocks // groups
    direct = devices <= chosen
    plan = (
        [("shift", shift, g * per_group) for shift in range(devices) for g in range(groups)]
        if direct
        else [("all", 0, 0)]
    )
    sends = [
        jax.ShapeDtypeStruct(
            (per_group if direct else devices * qblocks, KEY_BLOCK, 2 * LANES), BF16
        )
        for _ in plan
    ]
    chunk = 256
    kv_out = pl.pallas_call(
        functools.partial(kv_kernel, plan, devices, chunk),
        out_shape=[jax.ShapeDtypeStruct((per_device, KEY_BLOCK, 2 * LANES), BF16)] + sends,
        in_specs=[sm, sm, hb, hb, hb, vm, vm],
        out_specs=[vm] * (1 + len(sends)),
        scratch_shapes=[
            pltpu.VMEM((tok_count, width), BF16),
            pltpu.VMEM((width, 2 * LANES), BF16),
            pltpu.SemaphoreType.DMA((tok_count // chunk,)),
            pltpu.SemaphoreType.DMA((2,)),
        ],
        name="kv_project",
        cost_estimate=pl.CostEstimate(
            flops=2 * tok_count * width * 2 * LANES, bytes_accessed=4 * tok_count * width, transcendentals=0
        ),
    )(owner_t, part_t, tokens, key_weight, value_weight, coarse, fine)
    kv_rows, sent = kv_out[0], list(kv_out[1:])

    mine_owner = lax.dynamic_slice_in_dim(owner_t, me * qblocks, qblocks, 1)
    if direct:
        gathered = []
        for at, (_, shift, _) in enumerate(plan):
            if shift:
                pairs = [(i, i + shift) for i in range(devices - shift)]
                gathered.append(lax.ppermute(sent[at], "kv", pairs))
            else:
                gathered.append(sent[at])
        by_group = [gathered[g::groups] for g in range(groups)]
        wanted = me - jnp.arange(devices, dtype=jnp.int32)
        valid = jnp.any(mine_owner[:, :, None] == jnp.where(wanted < 0, -2, wanted), axis=0)
        valid = valid.astype(jnp.int32)
    else:
        got = lax.all_to_all(
            sent[0].reshape(devices, qblocks, KEY_BLOCK, 2 * LANES),
            "kv",
            split_axis=0,
            concat_axis=0,
            tiled=True,
        )
        rows = jnp.arange(qblocks, dtype=jnp.int32)
        picks = [got[jnp.maximum(mine_owner[slot], 0), rows] for slot in range(chosen)]
        by_group = [
            [p[g * per_group : (g + 1) * per_group] for p in picks] for g in range(groups)
        ]
        valid = (mine_owner.T >= 0).astype(jnp.int32)
    sources = valid.shape[1]

    q_rows = 256
    queries = pl.pallas_call(
        q_kernel,
        grid=(tok_count // q_rows,),
        out_shape=jax.ShapeDtypeStruct((tok_count, heads * LANES), BF16),
        in_specs=[
            pl.BlockSpec((1, q_rows, width), lambda i: (0, i, 0)),
            pl.BlockSpec((width, heads * HEAD_DIM), lambda i: (0, 0)),
            vm,
            vm,
        ],
        out_specs=pl.BlockSpec((q_rows, heads * LANES), lambda i: (i, 0)),
        name="q_project",
        cost_estimate=pl.CostEstimate(
            flops=2 * tok_count * width * heads * HEAD_DIM,
            bytes_accessed=4 * tok_count * width,
            transcendentals=0,
        ),
    )(tokens, query_weight, coarse, fine)
    other_weight = lax.ppermute(out_weight, "tp", swap)

    results = []
    gain = norm_gain.reshape(1, -1)
    cols = norm_gain.shape[0]
    depth = heads * HEAD_DIM
    for g in range(groups):
        at0 = g * per_group
        mixed = pl.pallas_call(
            functools.partial(attention_kernel, sources),
            grid=(per_group,),
            out_shape=jax.ShapeDtypeStruct((per_group * QUERY_BLOCK, depth), BF16),
            in_specs=[
                sm,
                pl.BlockSpec((QUERY_BLOCK, heads * LANES), lambda i, at0=at0: (at0 + i, 0)),
                pl.BlockSpec(
                    (QUERY_BLOCK // KEY_BLOCK, KEY_BLOCK, 2 * LANES), lambda i, at0=at0: (at0 + i, 0, 0)
                ),
            ]
            + [pl.BlockSpec((1, KEY_BLOCK, 2 * LANES), lambda i: (i, 0, 0))] * sources,
            out_specs=pl.BlockSpec((QUERY_BLOCK, depth), lambda i: (i, 0)),
            name=f"attend_{g}",
            cost_estimate=pl.CostEstimate(
                flops=4 * per_group * QUERY_BLOCK * heads * LANES * (sources * KEY_BLOCK + QUERY_BLOCK),
                bytes_accessed=per_group * QUERY_BLOCK * depth * 6,
                transcendentals=0,
            ),
        )(valid[at0 : at0 + per_group], queries, kv_rows, *by_group[g])
        other_mixed = lax.ppermute(mixed, "tp", swap)
        o_rows = 128
        results.append(
            pl.pallas_call(
                out_kernel,
                grid=(per_group * QUERY_BLOCK // o_rows,),
                out_shape=jax.ShapeDtypeStruct((per_group * QUERY_BLOCK, cols), BF16),
                in_specs=[
                    pl.BlockSpec((o_rows, depth), lambda i: (i, 0)),
                    pl.BlockSpec((o_rows, depth), lambda i: (i, 0)),
                    hb,
                    hb,
                    pl.BlockSpec((1, cols), lambda i: (0, 0)),
                ],
                out_specs=pl.BlockSpec((o_rows, cols), lambda i: (i, 0)),
                scratch_shapes=[
                    pltpu.VMEM((2, depth, 2 * cols), BF16),
                    pltpu.SemaphoreType.DMA((2, heads)),
                ],
                name=f"project_{g}",
                cost_estimate=pl.CostEstimate(
                    flops=8 * per_group * QUERY_BLOCK * depth * cols,
                    bytes_accessed=8 * depth * cols,
                    transcendentals=0,
                ),
            )(mixed, other_mixed, out_weight, other_weight, gain)
        )
    result = results[0] if groups == 1 else jnp.concatenate(results, axis=0)
    return result[None]


def solution(mesh):
    placed = (
        P("dp", "kv", None),
        P(None, "tp"),
        P(None, "tp"),
        P(None, "tp"),
        P("tp", None),
        P("tp"),
        P("dp", None, None),
        P("dp", None, None),
    )
    return jax.shard_map(
        body, mesh=mesh, in_specs=placed, out_specs=P("dp", "kv", "tp"), check_vma=False
    )
```

time: 118 us -> 51.7 us (0.44); the launches traced: 116 us -> 51.2 us
  local copies, waits for them, and re-layouts: 37.9 us -> 2.52 us
  Pallas kernels: 0 us -> 30.3 us
  matrix products: 25 us -> 0 us
  between operations: 13.6 us -> 0.07 us
  other arithmetic: 14.1 us -> 0.68 us
  starting transfers between devices: 9.07 us -> 5.46 us
  blocking collectives: 2.49 us -> 0 us
  waiting for transfers between devices: 13.8 us -> 12.1 us
    pallas_call x0 -> x4, Pallas kernels: none -> 30.3 us  [the longest x1 9.94 us: body(): pl.pallas_call(out_kernel, grid=(per_group * QUERY_BLOCK // o_rows,), out...]
    dot_general x5 -> x0, matrix products: 16.1 us -> none  [the longest x1 4.79 us: body(): jnp.einsum('bngqk,bknd->bqngd', weights, all_values, preferred_element_ty...]
    reduce_scatter x1 -> x0, waiting for transfers between devices: 13.8 us -> none  [body(): lax.psum_scatter(terms.astype(jnp.bfloat16), 'tp', scatter_dimension=1, t...]
    ppermute x0 -> x5, waiting for transfers between devices: none -> 12.1 us  [the longest x3 10 us: body(): gathered.append(lax.ppermute(sent[at], 'kv', pairs))]
    concatenate x6 -> x0, local copies, waits for them, and re-layouts: 11 us -> none  [rotate(): jnp.concatenate([first_half * cosine - second_half * sine_part, second_ha...]
    reshape x6 -> x0, local copies, waits for them, and re-layouts: 9.35 us -> none  [the longest x2 4.08 us: body(): picked_keys.reshape(qblocks, chosen_count * KEY_BLOCK, kv_here, HEAD_DIM)]
    all_to_all x2 -> x0, starting transfers between devices: 9.06 us -> none  [the longest x1 4.53 us: body(): lax.all_to_all(send_values, 'kv', split_axis=0, concat_axis=0, tiled=True)]
    sub x1 -> x0, matrix products: 8.85 us -> none  [body(): weights = jnp.exp(scores - row_max)]
  transfers between devices with their start and end apart: 3 -> 5, of which waited for: 1 -> 2; matrix products, arithmetic and copies ran while one was open for 31% -> 2% of each run, Pallas kernels for 0% -> 40%
where the time goes in v1:
time: 51.7 us; the launch traced here: 51.2 us
  Pallas kernels  30.3 us (59%)
  waiting for transfers between devices  12.1 us (23%)
  starting transfers between devices  5.46 us (11%)
  local copies, waits for them, and re-layouts  2.52 us (5%)
  other arithmetic  0.68 us (1%)
    ppermute x3, waiting for transfers between devices, body(): gathered.append(lax.ppermute(sent[at], 'kv', pairs))  10 us
    pallas_call x1, Pallas kernels, body(): pl.pallas_call(out_kernel, grid=(per_group * QUERY_BLOCK // o_rows,), out...  9.94 us
    pallas_call x1, Pallas kernels, body(): pl.pallas_call(functools.partial(attention_kernel, sources), grid=(per_gr...  8.3 us
    pallas_call x1, Pallas kernels, body(): pl.pallas_call(q_kernel, grid=(tok_count // q_rows,), out_shape=jax.Shape...  6.27 us
    pallas_call x1, Pallas kernels, body(): pl.pallas_call(functools.partial(kv_kernel, plan, devices, chunk), out_sh...  5.84 us
    ppermute x3, starting transfers between devices, body(): gathered.append(lax.ppermute(sent[at], 'kv', pairs))  3.88 us
    unnamed x12, local copies, waits for them, and re-layouts  2.33 us
    ppermute x1, waiting for transfers between devices, body(): other_mixed = lax.ppermute(mixed, 'tp', swap)  2.12 us
  transfers between devices with their start and end apart: 5, of which 2 were waited for; matrix products, arithmetic and copies ran while one was open for 2% of the time, Pallas kernels for 40%

profile of v1, /device:TPU:31, one launch (start us, length us, event | category | flops | bytes accessed | tf_op | source)
XLA Modules:
  0.0 51.2 jit_solution(11368117751134020610)
XLA Ops:
  0.0 0.7 %collective-permute-start.4 = (bf16[512,2048]{1,0:T(8,128)(2,1)}, bf16[512,2048]{1,0:T(8,128)(2,1)S(1)}, u32[]{:S(2)}, u32[]{:S(2)}) collective-permute-start(bf16[512,2048]{1,0:T(8,128)(2,1)} %w_mine_ref.1), channel_id=1, source_target_pairs={{0,1},{1,0},{2,3},{3,2},{4,5},{5,4},{6,7},{7,6},{8,9},{9,8},{10,11... | collective-permute-start | bytes 6291464 | tf_op jit(solution)/shard_map/ppermute | solution.py:314
  0.7 0.0 copy-start
  0.7 5.8 %kv_project.1 = (bf16[12,64,256]{2,1,0:T(8,128)(2,1)}, bf16[6,64,256]{2,1,0:T(8,128)(2,1)}, bf16[6,64,256]{2,1,0:T(8,128)(2,1)}, bf16[6,64,256]{2,1,0:T(8,128)(2,1)}, bf16[6,64,256]{2,1,0:T(8,128)(2,1)}) custom-call(s32[4,24]{1,0:T(4,128)} %bitcast.12, s32[4,24]{1,0:T(4,128)} %bitcast.13, bf16[1,768,2048]{2,1,0:T(8,128)(2,1)} %refs_2_.1, ...), custom_call_target="tpu_custom_call" | custom-call | flops 805306368 | bytes 6291456 | tf_op jit(solution)/shard_map/kv_project/pallas_call | solution.py:248
  6.5 1.3 %collective-permute-start = (bf16[6,64,256]{2,1,0:T(8,128)(2,1)}, bf16[6,64,256]{2,1,0:T(8,128)(2,1)S(1)}, u32[]{:S(2)}, u32[]{:S(2)}) collective-permute-start(bf16[6,64,256]{2,1,0:T(8,128)(2,1)} %get-tuple-element.12), channel_id=1, source_target_pairs={{0,2},{2,4},{4,6},{1,3},{3,5},{5,7},{8,10},{10,12},{12,14},{9,11},... | collective-permute-start | bytes 589832 | tf_op jit(solution)/shard_map/ppermute | solution.py:272
  7.8 1.3 %collective-permute-start.1 = (bf16[6,64,256]{2,1,0:T(8,128)(2,1)}, bf16[6,64,256]{2,1,0:T(8,128)(2,1)S(1)}, u32[]{:S(2)}, u32[]{:S(2)}) collective-permute-start(bf16[6,64,256]{2,1,0:T(8,128)(2,1)} %get-tuple-element.13), channel_id=1, source_target_pairs={{0,4},{2,6},{1,5},{3,7},{8,12},{10,14},{9,13},{11,15},{16,20},{18,... | collective-permute-start | bytes 589832 | tf_op jit(solution)/shard_map/ppermute | solution.py:272
  9.1 1.3 %collective-permute-start.2 = (bf16[6,64,256]{2,1,0:T(8,128)(2,1)}, bf16[6,64,256]{2,1,0:T(8,128)(2,1)S(1)}, u32[]{:S(2)}, u32[]{:S(2)}) collective-permute-start(bf16[6,64,256]{2,1,0:T(8,128)(2,1)} %get-tuple-element.14), channel_id=1, source_target_pairs={{0,6},{1,7},{8,14},{9,15},{16,22},{17,23},{24,30},{25,31}} | collective-permute-start | bytes 589832 | tf_op jit(solution)/shard_map/ppermute | solution.py:272
  10.4 0.0 copy-done
  10.5 0.1 dynamic-slice_bitcast_fusion
  10.5 0.1 compare_reduce_fusion
  10.6 0.1 copy.11
  10.7 0.6 %convert_element_type.3.valid_ref = s32[6,4]{1,0:T(8,128)} convert(pred[6,4]{1,0:T(8,128)(4,1)S(1)} %copy.11) | non-fusion elementwise | flops 24 | bytes 120 | tf_op jit(solution)/shard_map/convert_element_type | solution.py:278
  11.3 6.3 %q_project.1.q_ref = bf16[768,1024]{1,0:T(8,128)(2,1)} custom-call(bf16[1,768,2048]{2,1,0:T(8,128)(2,1)} %refs_2_.1, bf16[2048,512]{1,0:T(8,128)(2,1)} %wq_ref.1, f32[48,2,128]{2,1,0:T(2,128)} %constant.22.clone.coarse_ref.refs_5_, f32[2,64,128]{2,1,0:T(8,128)} %constant.23.clone.fine_ref.refs_6_), custom_call_target="tpu_custom_call" | custom-call | flops 1610612736 | bytes 6291456 | tf_op jit(solution)/shard_map/q_project/pallas_call | solution.py:296
  17.6 0.0 collective-permute-done.refs_1_
  17.6 0.0 copy-start.3
  17.6 10.0 %collective-permute-done.1.refs_2_ = bf16[6,64,256]{2,1,0:T(8,128)(2,1)S(1)} collective-permute-done((bf16[6,64,256]{2,1,0:T(8,128)(2,1)}, bf16[6,64,256]{2,1,0:T(8,128)(2,1)S(1)}, u32[]{:S(2)}, u32[]{:S(2)}) %collective-permute-start.1) | collective-permute-done | bytes 196640 | tf_op jit(solution)/shard_map/ppermute | solution.py:272
  27.6 0.0 copy-start.4
  27.6 0.0 collective-permute-done.2.refs_3_
  27.6 0.0 copy-start.5
  27.6 0.0 copy-done.3
  27.6 0.7 %copy-done.4 = bf16[6,64,256]{2,1,0:T(8,128)(2,1)} copy-done((bf16[6,64,256]{2,1,0:T(8,128)(2,1)}, bf16[6,64,256]{2,1,0:T(8,128)(2,1)S(1)}, u32[]{:S(2)}) %copy-start.4) | copy-done | bytes 196632
  28.3 0.1 copy-done.5
  28.4 8.3 %attend_0.1.mine_ref = bf16[768,512]{1,0:T(8,128)(2,1)} custom-call(s32[6,4]{1,0:T(8,128)} %convert_element_type.3.valid_ref, bf16[768,1024]{1,0:T(8,128)(2,1)} %q_project.1.q_ref, bf16[12,64,256]{2,1,0:T(8,128)(2,1)} %get-tuple-element.10.own_ref, bf16[6,64,256]{2,1,0:T(8,128)(2,1)} %get-tuple-element.11.refs_0_, bf16[6,64,256]{2,1,0:T(8,128)(2,1)} %copy-done.3, ...), custom_call_target="tpu_custom_call" | custom-call | flops 1207959552 | bytes 2359296 | tf_op jit(solution)/shard_map/attend_0/pallas_call | solution.py:322
  36.7 0.9 %collective-permute-start.3 = (bf16[768,512]{1,0:T(8,128)(2,1)}, bf16[768,512]{1,0:T(8,128)(2,1)S(1)}, u32[]{:S(2)}, u32[]{:S(2)}) collective-permute-start(bf16[768,512]{1,0:T(8,128)(2,1)} %attend_0.1.mine_ref), channel_id=1, source_target_pairs={{0,1},{1,0},{2,3},{3,2},{4,5},{5,4},{6,7},{7,6},{8,9},{9,8},{10,11... | collective-permute-start | bytes 2359304 | tf_op jit(solution)/shard_map/ppermute | solution.py:342
  37.6 2.1 %collective-permute-done.3.other_ref = bf16[768,512]{1,0:T(8,128)(2,1)S(1)} collective-permute-done((bf16[768,512]{1,0:T(8,128)(2,1)}, bf16[768,512]{1,0:T(8,128)(2,1)S(1)}, u32[]{:S(2)}, u32[]{:S(2)}) %collective-permute-start.3) | collective-permute-done | bytes 786464 | tf_op jit(solution)/shard_map/ppermute | solution.py:342
  39.7 0.0 copy-start.2
  39.7 0.0 collective-permute-done.4.w_other_ref
  39.7 0.0 copy-start.1
  39.7 0.9 %copy-done.2 = bf16[768,512]{1,0:T(8,128)(2,1)} copy-done((bf16[768,512]{1,0:T(8,128)(2,1)}, bf16[768,512]{1,0:T(8,128)(2,1)S(1)}, u32[]{:S(2)}) %copy-start.2) | copy-done | bytes 786456
  40.6 0.7 %copy-done.1 = bf16[512,2048]{1,0:T(8,128)(2,1)} copy-done((bf16[512,2048]{1,0:T(8,128)(2,1)}, bf16[512,2048]{1,0:T(8,128)(2,1)S(1)}, u32[]{:S(2)}) %copy-start.1) | copy-done | bytes 2097176
  41.3 9.9 %project_0.1 = bf16[768,1024]{1,0:T(8,128)(2,1)} custom-call(bf16[768,512]{1,0:T(8,128)(2,1)} %attend_0.1.mine_ref, bf16[768,512]{1,0:T(8,128)(2,1)} %copy-done.2, bf16[512,2048]{1,0:T(8,128)(2,1)} %w_mine_ref.1, bf16[512,2048]{1,0:T(8,128)(2,1)} %copy-done.1, f32[1,1024]{1,0:T(1,128)} %bitcast.14), custom_call_target="tpu_custom_call" | custom-call | flops 3221225472 | bytes 4194304 | tf_op jit(solution)/shard_map/project_0/pallas_call | solution.py:345
  (1 shorter events, 0.0 us)
Async XLA Ops:
  0.0 39.7 %collective-permute-start.4 = (bf16[512,2048]{1,0:T(8,128)(2,1)}, bf16[512,2048]{1,0:T(8,128)(2,1)S(1)}, u32[]{:S(2)}, u32[]{:S(2)}) collective-permute-start(bf16[512,2048]{1,0:T(8,128)(2,1)} %w_mine_ref.1), channel_id=1, source_target_pairs={{0,1},{1,0},{2,3},{3,2},{4,5},{5,4},{6,7},{7,6},{8,9},{9,8},{10,11... | collective-permute-start | bytes 6291464 | tf_op jit(solution)/shard_map/ppermute | solution.py:314
  0.7 9.8 %copy-start = (s32[1,24,4]{1,2,0:T(4,128)S(1)}, s32[1,24,4]{1,2,0:T(4,128)}, u32[]{:S(2)}) copy-start(s32[1,24,4]{1,2,0:T(4,128)} %param.16) | copy-start | bytes 1156
  6.5 11.1 %collective-permute-start = (bf16[6,64,256]{2,1,0:T(8,128)(2,1)}, bf16[6,64,256]{2,1,0:T(8,128)(2,1)S(1)}, u32[]{:S(2)}, u32[]{:S(2)}) collective-permute-start(bf16[6,64,256]{2,1,0:T(8,128)(2,1)} %get-tuple-element.12), channel_id=1, source_target_pairs={{0,2},{2,4},{4,6},{1,3},{3,5},{5,7},{8,10},{10,12},{12,14},{9,11},... | collective-permute-start | bytes 589832 | tf_op jit(solution)/shard_map/ppermute | solution.py:272
  7.8 19.8 %collective-permute-start.1 = (bf16[6,64,256]{2,1,0:T(8,128)(2,1)}, bf16[6,64,256]{2,1,0:T(8,128)(2,1)S(1)}, u32[]{:S(2)}, u32[]{:S(2)}) collective-permute-start(bf16[6,64,256]{2,1,0:T(8,128)(2,1)} %get-tuple-element.13), channel_id=1, source_target_pairs={{0,4},{2,6},{1,5},{3,7},{8,12},{10,14},{9,13},{11,15},{16,20},{18,... | collective-permute-start | bytes 589832 | tf_op jit(solution)/shard_map/ppermute | solution.py:272
  9.1 18.5 %collective-permute-start.2 = (bf16[6,64,256]{2,1,0:T(8,128)(2,1)}, bf16[6,64,256]{2,1,0:T(8,128)(2,1)S(1)}, u32[]{:S(2)}, u32[]{:S(2)}) collective-permute-start(bf16[6,64,256]{2,1,0:T(8,128)(2,1)} %get-tuple-element.14), channel_id=1, source_target_pairs={{0,6},{1,7},{8,14},{9,15},{16,22},{17,23},{24,30},{25,31}} | collective-permute-start | bytes 589832 | tf_op jit(solution)/shard_map/ppermute | solution.py:272
  17.6 10.0 %copy-start.3 = (bf16[6,64,256]{2,1,0:T(8,128)(2,1)}, bf16[6,64,256]{2,1,0:T(8,128)(2,1)S(1)}, u32[]{:S(2)}) copy-start(bf16[6,64,256]{2,1,0:T(8,128)(2,1)S(1)} %collective-permute-done.refs_1_) | copy-start | bytes 589828
  27.6 0.7 %copy-start.4 = (bf16[6,64,256]{2,1,0:T(8,128)(2,1)}, bf16[6,64,256]{2,1,0:T(8,128)(2,1)S(1)}, u32[]{:S(2)}) copy-start(bf16[6,64,256]{2,1,0:T(8,128)(2,1)S(1)} %collective-permute-done.1.refs_2_) | copy-start | bytes 589828
  27.6 0.8 %copy-start.5 = (bf16[6,64,256]{2,1,0:T(8,128)(2,1)}, bf16[6,64,256]{2,1,0:T(8,128)(2,1)S(1)}, u32[]{:S(2)}) copy-start(bf16[6,64,256]{2,1,0:T(8,128)(2,1)S(1)} %collective-permute-done.2.refs_3_) | copy-start | bytes 589828
  36.7 3.0 %collective-permute-start.3 = (bf16[768,512]{1,0:T(8,128)(2,1)}, bf16[768,512]{1,0:T(8,128)(2,1)S(1)}, u32[]{:S(2)}, u32[]{:S(2)}) collective-permute-start(bf16[768,512]{1,0:T(8,128)(2,1)} %attend_0.1.mine_ref), channel_id=1, source_target_pairs={{0,1},{1,0},{2,3},{3,2},{4,5},{5,4},{6,7},{7,6},{8,9},{9,8},{10,11... | collective-permute-start | bytes 2359304 | tf_op jit(solution)/shard_map/ppermute | solution.py:342
  39.7 0.9 %copy-start.2 = (bf16[768,512]{1,0:T(8,128)(2,1)}, bf16[768,512]{1,0:T(8,128)(2,1)S(1)}, u32[]{:S(2)}) copy-start(bf16[768,512]{1,0:T(8,128)(2,1)S(1)} %collective-permute-done.3.other_ref) | copy-start | bytes 2359300
  39.7 1.6 %copy-start.1 = (bf16[512,2048]{1,0:T(8,128)(2,1)}, bf16[512,2048]{1,0:T(8,128)(2,1)S(1)}, u32[]{:S(2)}) copy-start(bf16[512,2048]{1,0:T(8,128)(2,1)S(1)} %collective-permute-done.4.w_other_ref) | copy-start | bytes 6291460

commit v2 on v1

v2 whole, which is shorter than its diff:
```python
import functools

import jax
import jax.numpy as jnp
import numpy as np
from jax import lax
from jax.experimental import pallas as pl
from jax.experimental.pallas import tpu as pltpu
from jax.sharding import PartitionSpec as P


HEAD_DIM = 64
QUERY_BLOCK = 128
KEY_BLOCK = 64
LANES = 128
ROPE_BASE = 10000.0
NORM_EPS = 1e-06
LOG2E = 1.4426950408889634
GROUPS = (3, 3)
PER_DOT = 2
OUT_SPLIT = 2


BF16 = jnp.bfloat16
F32 = jnp.float32
HBM = pltpu.MemorySpace.HBM
VMEM = pltpu.MemorySpace.VMEM


def angle_tables(length):
    half = HEAD_DIM // 2
    frequency = ROPE_BASE ** (-np.arange(half, dtype=np.float64) / half)
    lane_frequency = np.tile(frequency, LANES // half)
    sign = np.tile(np.repeat([-1.0, 1.0], half), LANES // HEAD_DIM)
    coarse = (np.arange(length // KEY_BLOCK) * KEY_BLOCK)[:, None] * lane_frequency
    fine = np.arange(KEY_BLOCK)[:, None] * lane_frequency
    make = lambda a: np.stack([np.cos(a), np.sin(a) * sign], 1).astype(np.float32)
    return make(coarse), np.swapaxes(make(fine), 0, 1).copy()


def rotate_tile(tile, cosine, sine):
    lane = lax.broadcasted_iota(jnp.int32, tile.shape, 1)
    half = HEAD_DIM // 2
    first = (lane % HEAD_DIM) < half
    swapped = jnp.where(
        first, pltpu.roll(tile, LANES - half, 1), pltpu.roll(tile, half, 1)
    )
    return tile * cosine + swapped * sine


def block_angles(coarse_ref, fine_ref, block):
    coarse = coarse_ref[block]
    c_a, s_a = coarse[0:1], coarse[1:2]
    c_b, s_b = fine_ref[0], fine_ref[1]
    return c_a * c_b - s_a * s_b, s_a * c_b + c_a * s_b


def wanted_block(owner_ref, part_ref, row, me):
    total = jnp.int32(0)
    for slot in range(owner_ref.shape[0]):
        total = total + jnp.where(owner_ref[slot, row] == me, part_ref[slot, row], 0)
    return total


def kv_kernel(plan, chunk, *refs):
    owner_hbm, part_hbm, tokens_ref, wk_ref, wv_ref, coarse_hbm, fine_hbm = refs[:7]
    kv_ref, bias_ref, tok = refs[7:10]
    send_refs = refs[10 : 10 + len(plan)]
    weight, coarse_ref, fine_ref, owner_ref, part_ref, tok_sem, sem = refs[10 + len(plan) :]
    rows = tok.shape[0]
    me = lax.axis_index("kv")
    per_chunk = chunk // KEY_BLOCK
    blocks = rows // KEY_BLOCK
    qblocks = rows // QUERY_BLOCK
    small = [
        (wk_ref, weight.at[:, pl.ds(0, LANES)]),
        (wv_ref, weight.at[:, pl.ds(LANES, LANES)]),
        (coarse_hbm.at[pl.ds(me * blocks, blocks)], coarse_ref),
        (fine_hbm, fine_ref),
        (owner_hbm, owner_ref),
        (part_hbm, part_ref),
    ]
    small = [pltpu.make_async_copy(src, dst, sem.at[at]) for at, (src, dst) in enumerate(small)]
    t_copies = [
        pltpu.make_async_copy(
            tokens_ref.at[0, pl.ds(at * chunk, chunk)], tok.at[pl.ds(at * chunk, chunk)], tok_sem.at[at]
        )
        for at in range(rows // chunk)
    ]
    for copy in small[:2] + t_copies[:1] + small[2:] + t_copies[1:]:
        copy.start()
    for copy in small:
        copy.wait()
    for at in range(rows // chunk):
        t_copies[at].wait()
        product = jnp.dot(
            tok[pl.ds(at * chunk, chunk)], weight[...], preferred_element_type=F32
        )
        for sub in range(per_chunk):
            block = at * per_chunk + sub
            cosine, sine = block_angles(coarse_ref, fine_ref, block)
            piece = product[sub * KEY_BLOCK : (sub + 1) * KEY_BLOCK]
            kv_ref[block, :, 0:LANES] = rotate_tile(piece[:, :LANES], cosine, sine).astype(BF16)
            kv_ref[block, :, LANES : 2 * LANES] = piece[:, LANES:].astype(BF16)
    for (kind, arg, first), out in zip(plan, send_refs):
        if kind == "pair":
            target = me ^ arg
            for row in range(out.shape[0]):
                out[row] = kv_ref[wanted_block(owner_ref, part_ref, target * qblocks + first + row, me)]
        else:
            def fill(index, carry, out=out):
                out[index] = kv_ref[wanted_block(owner_ref, part_ref, index, me)]
                return carry
            lax.fori_loop(0, out.shape[0], fill, 0)
    far = bias_ref.shape[2]
    source_id = lax.broadcasted_iota(jnp.int32, (1, far), 1) // KEY_BLOCK
    for row in range(qblocks):
        owners = [owner_ref[slot, me * qblocks + row] for slot in range(owner_ref.shape[0])]
        if plan[0][0] == "pair":
            wanted = me ^ source_id
            named = functools.reduce(
                jnp.logical_or, [wanted == owner for owner in owners]
            )
        else:
            named = functools.reduce(
                jnp.logical_or,
                [jnp.logical_and(source_id == at, owner >= 0) for at, owner in enumerate(owners)],
            )
        bias_ref[row] = jnp.where(named, jnp.float32(0), jnp.float32(-jnp.inf))


def q_kernel(chunk, tok_ref, weight_ref, coarse_ref, fine_ref, out_ref):
    rows, tiles = tok_ref.shape[0], weight_ref.shape[1] // LANES
    blocks = rows // KEY_BLOCK
    me = lax.axis_index("kv")
    low = lax.broadcasted_iota(jnp.int32, (KEY_BLOCK, LANES), 1) < HEAD_DIM
    per_chunk = chunk // KEY_BLOCK
    for at in range(rows // chunk):
        product = jnp.dot(
            tok_ref[at * chunk : (at + 1) * chunk], weight_ref[...], preferred_element_type=F32
        ) * (HEAD_DIM ** -0.5)
        for sub in range(per_chunk):
            block = at * per_chunk + sub
            cosine, sine = block_angles(coarse_ref, fine_ref, me * blocks + block)
            span = slice(block * KEY_BLOCK, (block + 1) * KEY_BLOCK)
            for tile in range(tiles):
                piece = rotate_tile(
                    product[sub * KEY_BLOCK : (sub + 1) * KEY_BLOCK, tile * LANES : (tile + 1) * LANES],
                    cosine,
                    sine,
                )
                other = pltpu.roll(piece, HEAD_DIM, 1)
                if tile < tiles // 2:
                    even, odd = jnp.where(low, piece, 0.0), jnp.where(low, other, 0.0)
                else:
                    even, odd = jnp.where(low, 0.0, other), jnp.where(low, 0.0, piece)
                out_ref[2 * tile, span] = even.astype(BF16)
                out_ref[2 * tile + 1, span] = odd.astype(BF16)


def attention_kernel(first, sources, per_dot, q_ref, own_ref, bias_ref, *refs):
    source_refs, out_ref = refs[:sources], refs[-1]
    heads = q_ref.shape[0]
    pairs = heads // 2
    far = sources * KEY_BLOCK
    row_id = lax.broadcasted_iota(jnp.int32, (QUERY_BLOCK, QUERY_BLOCK), 0)
    col_id = lax.broadcasted_iota(jnp.int32, (QUERY_BLOCK, QUERY_BLOCK), 1)
    lower = row_id >= col_id
    low = lax.broadcasted_iota(jnp.int32, (QUERY_BLOCK, LANES), 1) < HEAD_DIM
    per_query = QUERY_BLOCK // KEY_BLOCK
    for row in range(out_ref.shape[0] // QUERY_BLOCK):
        block = first + row
        picks = [ref[row] for ref in source_refs]
        picks += [own_ref[block * per_query + at] for at in range(per_query)]
        keys = jnp.concatenate([p[:, :LANES] for p in picks], axis=0)
        values = jnp.concatenate([p[:, LANES:] for p in picks], axis=0)
        values = jnp.concatenate([values, jnp.ones_like(values)], axis=1)
        bias = bias_ref[block]
        span = pl.ds(block * QUERY_BLOCK, QUERY_BLOCK)
        for start in range(0, pairs, per_dot):
            order = [h for p in range(start, start + per_dot) for h in (p, p + pairs)]
            query = jnp.concatenate([q_ref[h, span] for h in order], axis=0)
            scores = lax.dot_general(
                query, keys, (((1,), (1,)), ((), ())), preferred_element_type=F32
            )
            parts = []
            for at in range(len(order)):
                piece = scores[at * QUERY_BLOCK : (at + 1) * QUERY_BLOCK]
                piece = jnp.concatenate(
                    [piece[:, :far] + bias, jnp.where(lower, piece[:, far:], -jnp.inf)], axis=1
                )
                row_max = jnp.max(piece, axis=1, keepdims=True)
                parts.append(jnp.exp2((piece - row_max) * LOG2E).astype(BF16))
            mixed = jnp.dot(jnp.concatenate(parts, axis=0), values, preferred_element_type=F32)
            for at in range(per_dot):
                one = mixed[2 * at * QUERY_BLOCK : (2 * at + 1) * QUERY_BLOCK]
                two = mixed[(2 * at + 1) * QUERY_BLOCK : (2 * at + 2) * QUERY_BLOCK]
                top = jnp.where(low, one[:, :LANES], two[:, :LANES])
                bottom = jnp.where(low, one[:, LANES:], two[:, LANES:])
                out_ref[
                    row * QUERY_BLOCK : (row + 1) * QUERY_BLOCK, (start + at) * LANES : (start + at + 1) * LANES
                ] = (top / bottom).astype(BF16)


def out_kernel(first, split, mine_ref, other_ref, w_mine_ref, w_other_ref, gain_ref, *refs):
    out_hbm, kept, staged, sem = refs[-4:]
    rows, cols = staged.shape
    depth = w_mine_ref.shape[0]
    heads = depth // HEAD_DIM
    me = lax.axis_index("tp")
    width = 256
    order = [h for p in range(heads // 2) for h in (p, p + heads // 2)]
    tile = rows // split
    copies = []
    for part in range(split):
        span = slice(part * tile, (part + 1) * tile)
        mine, other = mine_ref[span], other_ref[span]
        total = None
        for half in range(2):
            for at in range(cols // width):
                start = pl.multiple_of((me if half == 0 else 1 - me) * cols + at * width, width)
                load = lambda ref: jnp.concatenate(
                    [ref[h * HEAD_DIM : (h + 1) * HEAD_DIM, pl.ds(start, width)] for h in order], axis=0
                )
                a = jnp.dot(mine, load(w_mine_ref), preferred_element_type=F32)
                b = jnp.dot(other, load(w_other_ref), preferred_element_type=F32)
                projected = a.astype(BF16).astype(F32) + b.astype(BF16).astype(F32)
                if half == 0:
                    kept[span, at * width : (at + 1) * width] = projected
                squares = projected * projected
                squares = squares[:, :LANES] + squares[:, LANES:]
                total = squares if total is None else total + squares
        total = jnp.sum(total, axis=1, keepdims=True)
        scale = lax.rsqrt(total / (2 * cols) + NORM_EPS)
        for at in range(cols // width):
            put = slice(at * width, (at + 1) * width)
            staged[span, put] = (kept[span, put] * scale * gain_ref[:, put]).astype(BF16)
        copies.append(
            pltpu.make_async_copy(
                staged.at[pl.ds(part * tile, tile)],
                out_hbm.at[0, pl.ds(first * QUERY_BLOCK + part * tile, tile)],
                sem.at[part],
            )
        )
        copies[-1].start()
    for copy in copies:
        copy.wait()


def body(
    tokens, query_weight, key_weight, value_weight, out_weight, norm_gain, chosen_owner, chosen_part
):
    tok_count, width = tokens.shape[1], tokens.shape[2]
    devices = lax.axis_size("kv")
    me = lax.axis_index("kv")
    heads = query_weight.shape[1] // HEAD_DIM
    assert key_weight.shape[1] == LANES and value_weight.shape[1] == LANES
    per_device = tok_count // KEY_BLOCK
    qblocks = tok_count // QUERY_BLOCK
    owner_t, part_t = chosen_owner[0].T, chosen_part[0].T
    chosen = owner_t.shape[0]
    coarse, fine = (jnp.asarray(t) for t in angle_tables(devices * tok_count))
    swap = [(0, 1), (1, 0)]
    vm = pl.BlockSpec(memory_space=VMEM)
    hb = pl.BlockSpec(memory_space=HBM)
    direct = devices <= chosen and devices & (devices - 1) == 0
    resident = functools.partial(pltpu.with_memory_space_constraint, memory_space=VMEM)
    distant = functools.partial(pltpu.with_memory_space_constraint, memory_space=HBM)

    sizes = GROUPS if direct and sum(GROUPS) == qblocks else (qblocks,)
    firsts = [sum(sizes[:g]) for g in range(len(sizes))]
    sources = devices if direct else chosen
    plan = (
        [("pair", pair, firsts[g]) for g in range(len(sizes)) for pair in range(devices)]
        if direct
        else [("all", 0, 0)]
    )
    block_shape = (KEY_BLOCK, 2 * LANES)
    sends = (
        [pltpu.VMEM((sizes[g],) + block_shape, BF16) for g in range(len(sizes)) for _ in range(devices)]
        if direct
        else [jax.ShapeDtypeStruct((devices * qblocks,) + block_shape, BF16)]
    )
    chunk = 256
    table_scratch = [pltpu.VMEM((per_device, 2, LANES), F32), pltpu.VMEM((2, KEY_BLOCK, LANES), F32)]
    kv_out = pl.pallas_call(
        functools.partial(kv_kernel, plan, chunk),
        out_shape=[
            pltpu.VMEM((per_device,) + block_shape, BF16),
            pltpu.VMEM((qblocks, 1, sources * KEY_BLOCK), F32),
            pltpu.VMEM((tok_count, width), BF16),
        ]
        + sends,
        in_specs=[hb] * 7,
        out_specs=[vm] * (3 + len(sends)),
        scratch_shapes=[
            pltpu.VMEM((width, 2 * LANES), BF16),
            *table_scratch,
            pltpu.SMEM(owner_t.shape, jnp.int32),
            pltpu.SMEM(part_t.shape, jnp.int32),
            pltpu.SemaphoreType.DMA((tok_count // chunk,)),
            pltpu.SemaphoreType.DMA((6,)),
        ],
        compiler_params=pltpu.CompilerParams(vmem_limit_bytes=24 << 20),
        name="kv_project",
        cost_estimate=pl.CostEstimate(
            flops=2 * tok_count * width * 2 * LANES, bytes_accessed=4 * tok_count * width, transcendentals=0
        ),
    )(*map(distant, (owner_t, part_t, tokens, key_weight, value_weight, coarse, fine)))
    kv_rows, bias, loaded, sent = kv_out[0], kv_out[1], kv_out[2], list(kv_out[3:])

    if direct:
        by_group = []
        for g in range(len(sizes)):
            arrived = []
            for pair in range(devices):
                block = sent[g * devices + pair]
                if pair:
                    block = lax.ppermute(block, "kv", [(i, i ^ pair) for i in range(devices)])
                arrived.append(resident(block))
            by_group.append(arrived)
    else:
        got = lax.all_to_all(
            sent[0].reshape((devices, qblocks) + block_shape), "kv", split_axis=0, concat_axis=0, tiled=True
        )
        mine_owner = lax.dynamic_slice_in_dim(owner_t, me * qblocks, qblocks, 1)
        rows = jnp.arange(qblocks, dtype=jnp.int32)
        by_group = [[got[jnp.maximum(mine_owner[slot], 0), rows] for slot in range(chosen)]]

    queries = pl.pallas_call(
        functools.partial(q_kernel, chunk),
        out_shape=pltpu.VMEM((heads, tok_count, LANES), BF16),
        in_specs=[vm] * 4,
        out_specs=vm,
        compiler_params=pltpu.CompilerParams(vmem_limit_bytes=24 << 20),
        name="q_project",
        cost_estimate=pl.CostEstimate(
            flops=2 * tok_count * width * heads * HEAD_DIM,
            bytes_accessed=4 * tok_count * width,
            transcendentals=0,
        ),
    )(*map(resident, (loaded, query_weight, coarse, fine)))
    other_weight = resident(lax.ppermute(out_weight, "tp", swap))
    my_weight = resident(out_weight)

    gain = norm_gain.reshape(1, -1)
    cols = norm_gain.shape[0]
    depth = heads * HEAD_DIM
    result = None
    for g, (first, size) in enumerate(zip(firsts, sizes)):
        tokens_here = size * QUERY_BLOCK
        extra = [] if result is None else [result]
        mixed = pl.pallas_call(
            functools.partial(attention_kernel, first, sources, PER_DOT),
            out_shape=pltpu.VMEM((tokens_here, depth), BF16),
            in_specs=[vm] * (3 + sources) + [hb] * len(extra),
            out_specs=vm,
            compiler_params=pltpu.CompilerParams(vmem_limit_bytes=24 << 20),
            cost_estimate=pl.CostEstimate(
                flops=4 * tokens_here * heads * LANES * (sources * KEY_BLOCK + QUERY_BLOCK),
                bytes_accessed=tokens_here * depth * 6,
                transcendentals=0,
            ),
        )(resident(queries), resident(kv_rows), resident(bias), *by_group[g], *map(distant, extra))
        other_mixed = resident(lax.ppermute(mixed, "tp", swap))
        split = OUT_SPLIT
        result = pl.pallas_call(
            functools.partial(out_kernel, first, split),
            out_shape=jax.ShapeDtypeStruct((1, tok_count, cols), BF16),
            in_specs=[vm, vm, vm, vm, vm] + [hb] * len(extra),
            out_specs=hb,
            input_output_aliases={5: 0} if extra else {},
            scratch_shapes=[
                pltpu.VMEM((tokens_here, cols), F32),
                pltpu.VMEM((tokens_here, cols), BF16),
                pltpu.SemaphoreType.DMA((split,)),
            ],
            compiler_params=pltpu.CompilerParams(vmem_limit_bytes=24 << 20),
            cost_estimate=pl.CostEstimate(
                flops=8 * tokens_here * depth * cols,
                bytes_accessed=8 * depth * cols,
                transcendentals=0,
            ),
        )(resident(mixed), other_mixed, my_weight, other_weight, gain, *map(distant, extra))
    return result


def solution(mesh):
    placed = (
        P("dp", "kv", None),
        P(None, "tp"),
        P(None, "tp"),
        P(None, "tp"),
        P("tp", None),
        P("tp"),
        P("dp", None, None),
        P("dp", None, None),
    )
    return jax.shard_map(body, mesh=mesh, in_specs=placed, out_specs=P("dp", "kv", "tp"), check_vma=False)
```

time: 51.7 us -> 40.4 us (0.78)
  the two profiles are of different devices: /device:TPU:31 before, /device:TPU:0 now
where the time goes in v2:
time: 40.4 us; the launch traced here: 40.3 us
  Pallas kernels  16.9 us (42%)
  waiting for transfers between devices  12.9 us (32%)
  starting transfers between devices  10.4 us (26%)
    ppermute x6, waiting for transfers between devices, body(): block = lax.ppermute(block, 'kv', [(i, i ^ pair) for i in range(devices)])  11.2 us
    ppermute x6, starting transfers between devices, body(): block = lax.ppermute(block, 'kv', [(i, i ^ pair) for i in range(devices)])  9.73 us
    pallas_call x2, Pallas kernels, body(): pl.pallas_call(functools.partial(out_kernel, first, split), out_shape=jax...  6.02 us
    pallas_call x2, Pallas kernels, body(): pl.pallas_call(functools.partial(attention_kernel, first, sources, PER_DO...  4.61 us
    pallas_call x1, Pallas kernels, body(): pl.pallas_call(functools.partial(kv_kernel, plan, chunk), out_shape=[pltp...  4.14 us
    pallas_call x1, Pallas kernels, body(): pl.pallas_call(functools.partial(q_kernel, chunk), out_shape=pltpu.VMEM((...  2.14 us
    ppermute x2, waiting for transfers between devices, body(): other_mixed = resident(lax.ppermute(mixed, 'tp', swap))  1.71 us
  transfers between devices with their start and end apart: 9, of which 3 were waited for; matrix products, arithmetic and copies ran while one was open for 0% of the time, Pallas kernels for 29%

profile of v2, /device:TPU:0, one launch (start us, length us, event | category | flops | bytes accessed | tf_op | source)
XLA Modules:
  0.0 40.3 jit_solution(892234032855367008)
XLA Ops:
  0.0 0.5 %collective-permute-start.7 = (bf16[512,2048]{1,0:T(8,128)(2,1)}, bf16[512,2048]{1,0:T(8,128)(2,1)S(1)}, u32[]{:S(2)}, u32[]{:S(2)}) collective-permute-start(bf16[512,2048]{1,0:T(8,128)(2,1)} %w_mine_ref.3), channel_id=1, source_target_pairs={{0,1},{1,0},{2,3},{3,2},{4,5},{5,4},{6,7},{7,6},{8,9},{9,8},{10,11... | collective-permute-start | bytes 6291464 | tf_op jit(solution)/shard_map/ppermute | solution.py:343
  0.5 0.0 copy-start.1
  0.5 0.0 copy-start.2
  0.5 0.0 copy-start.3
  0.5 4.1 %kv_project.1 = (bf16[12,64,256]{2,1,0:T(8,128)(2,1)S(1)}, f32[6,1,256]{2,1,0:T(1,128)S(1)}, bf16[768,2048]{1,0:T(8,128)(2,1)S(1)}, bf16[3,64,256]{2,1,0:T(8,128...) custom-call(s32[4,24]{1,0:T(4,128)} %bitcast.9, ...), custom_call_target="tpu_custom_call" | custom-call | flops 805306368 | bytes 6291456 | tf_op jit(solution)/shard_map/kv_project/pallas_call | solution.py:286
  4.6 2.7 %collective-permute-start.3 = (bf16[3,64,256]{2,1,0:T(8,128)(2,1)S(1)}, bf16[3,64,256]{2,1,0:T(8,128)(2,1)S(1)}, u32[]{:S(2)}, u32[]{:S(2)}) collective-permute-start(bf16[3,64,256]{2,1,0:T(8,128)(2,1)S(1)} %get-tuple-element.24), channel_id=1, source_target_pairs={{0,2},{2,0},{4,6},{6,4},{1,3},{3,1},{5,7},{7,5},{8,10},{10,8},{12,... | collective-permute-start | bytes 294920 | tf_op jit(solution)/shard_map/ppermute | solution.py:319
  7.3 2.6 %collective-permute-start.4 = (bf16[3,64,256]{2,1,0:T(8,128)(2,1)S(1)}, bf16[3,64,256]{2,1,0:T(8,128)(2,1)S(1)}, u32[]{:S(2)}, u32[]{:S(2)}) collective-permute-start(bf16[3,64,256]{2,1,0:T(8,128)(2,1)S(1)} %get-tuple-element.25), channel_id=1, source_target_pairs={{0,4},{2,6},{4,0},{6,2},{1,5},{3,7},{5,1},{7,3},{8,12},{10,14},{12... | collective-permute-start | bytes 294920 | tf_op jit(solution)/shard_map/ppermute | solution.py:319
  9.9 0.0 collective-permute-start.5
  9.9 0.0 copy-done.1
  9.9 0.0 copy-done.2
  9.9 0.0 copy-done.3
  9.9 2.1 %q_project.1.q_ref = bf16[8,768,128]{2,1,0:T(8,128)(2,1)S(1)} custom-call(bf16[768,2048]{1,0:T(8,128)(2,1)S(1)} %get-tuple-element.16.tok_ref, bf16[2048,512]{1,0:T(8,128)(2,1)S(1)} %copy-done.1, f32[48,2,128]{2,1,0:T(2,128)S(1)} %copy-done.3, f32[2,64,128]{2,1,0:T(8,128)S(1)} %copy-done.2), custom_call_target="tpu_custom_call" | custom-call | flops 1610612736 | bytes 6291456 | tf_op jit(solution)/shard_map/q_project/pallas_call | solution.py:330
  12.1 0.0 copy-start
  12.1 0.0 copy-start.4
  12.1 0.0 collective-permute-done.3.refs_1_
  12.1 6.0 %collective-permute-done.4.refs_2_ = bf16[3,64,256]{2,1,0:T(8,128)(2,1)S(1)} collective-permute-done((bf16[3,64,256]{2,1,0:T(8,128)(2,1)S(1)}, bf16[3,64,256]{2,1,0:T(8,128)(2,1)S(1)}, u32[]{:S(2)}, u32[]{:S(2)}) %collective-permute-start.4) | collective-permute-done | bytes 98336 | tf_op jit(solution)/shard_map/ppermute | solution.py:319
  18.1 0.0 collective-permute-done.5.refs_3_
  18.1 2.3 %shard_map.100.mine_ref = bf16[384,512]{1,0:T(8,128)(2,1)S(1)} custom-call(bf16[8,768,128]{2,1,0:T(8,128)(2,1)S(1)} %q_project.1.q_ref, bf16[12,64,256]{2,1,0:T(8,128)(2,1)S(1)} %get-tuple-element.17.own_ref, f32[6,1,256]{2,1,0:T(1,128)S(1)} %get-tuple-element.18.bias_ref, bf16[3,64,256]{2,1,0:T(8,128)(2,1)S(1)} %get-tuple-element.23.refs_0_, ...), custom_call_target="tpu_custom_call" | custom-call | flops 603979776 | bytes 1179648 | tf_op jit(solution)/shard_map/pallas_call | solution.py:353
  20.4 0.1 collective-permute-start.6
  20.5 2.0 %collective-permute-start = (bf16[3,64,256]{2,1,0:T(8,128)(2,1)S(1)}, bf16[3,64,256]{2,1,0:T(8,128)(2,1)S(1)}, u32[]{:S(2)}, u32[]{:S(2)}) collective-permute-start(bf16[3,64,256]{2,1,0:T(8,128)(2,1)S(1)} %get-tuple-element.20), channel_id=1, source_target_pairs={{0,2},{2,0},{4,6},{6,4},{1,3},{3,1},{5,7},{7,5},{8,10},{10,8},{12,... | collective-permute-start | bytes 294920 | tf_op jit(solution)/shard_map/ppermute | solution.py:319
  22.4 1.2 %collective-permute-start.1 = (bf16[3,64,256]{2,1,0:T(8,128)(2,1)S(1)}, bf16[3,64,256]{2,1,0:T(8,128)(2,1)S(1)}, u32[]{:S(2)}, u32[]{:S(2)}) collective-permute-start(bf16[3,64,256]{2,1,0:T(8,128)(2,1)S(1)} %get-tuple-element.21), channel_id=1, source_target_pairs={{0,4},{2,6},{4,0},{6,2},{1,5},{3,7},{5,1},{7,3},{8,12},{10,14},{12... | collective-permute-start | bytes 294920 | tf_op jit(solution)/shard_map/ppermute | solution.py:319
  23.6 1.3 %collective-permute-start.2 = (bf16[3,64,256]{2,1,0:T(8,128)(2,1)S(1)}, bf16[3,64,256]{2,1,0:T(8,128)(2,1)S(1)}, u32[]{:S(2)}, u32[]{:S(2)}) collective-permute-start(bf16[3,64,256]{2,1,0:T(8,128)(2,1)S(1)} %get-tuple-element.22), channel_id=1, source_target_pairs={{0,6},{2,4},{4,2},{6,0},{1,7},{3,5},{5,3},{7,1},{8,14},{10,12},{12... | collective-permute-start | bytes 294920 | tf_op jit(solution)/shard_map/ppermute | solution.py:319
  25.0 0.0 collective-permute-done.6.other_ref
  25.0 0.0 collective-permute-done.7.w_other_ref
  25.0 0.0 copy-done
  25.0 0.0 copy-done.4
  25.0 3.0 %shard_map.101.refs_4_.refs_0_ = bf16[1,768,1024]{2,1,0:T(8,128)(2,1)} custom-call(bf16[384,512]{1,0:T(8,128)(2,1)S(1)} %shard_map.100.mine_ref, bf16[384,512]{1,0:T(8,128)(2,1)S(1)} %collective-permute-done.6.other_ref, bf16[512,2048]{1,0:T(8,128)(2,1)S(1)} %copy-done, bf16[512,2048]{1,0:T(8,128)(2,1)S(1)} %collective-permute-done.7.w_other_ref, ...), custom_call_target="tpu_custom_call" | custom-call | flops 1610612736 | bytes 4194304 | tf_op jit(solution)/shard_map/pallas_call | solution.py:367
  28.0 0.0 collective-permute-done.refs_1_
  28.0 5.2 %collective-permute-done.1.refs_2_ = bf16[3,64,256]{2,1,0:T(8,128)(2,1)S(1)} collective-permute-done((bf16[3,64,256]{2,1,0:T(8,128)(2,1)S(1)}, bf16[3,64,256]{2,1,0:T(8,128)(2,1)S(1)}, u32[]{:S(2)}, u32[]{:S(2)}) %collective-permute-start.1) | collective-permute-done | bytes 98336 | tf_op jit(solution)/shard_map/ppermute | solution.py:319
  33.2 0.0 collective-permute-done.2.refs_3_
  33.2 2.3 %shard_map.102.mine_ref = bf16[384,512]{1,0:T(8,128)(2,1)S(1)} custom-call(bf16[8,768,128]{2,1,0:T(8,128)(2,1)S(1)} %q_project.1.q_ref, bf16[12,64,256]{2,1,0:T(8,128)(2,1)S(1)} %get-tuple-element.17.own_ref, f32[6,1,256]{2,1,0:T(1,128)S(1)} %get-tuple-element.18.bias_ref, bf16[3,64,256]{2,1,0:T(8,128)(2,1)S(1)} %get-tuple-element.19.refs_0_, ...), custom_call_target="tpu_custom_call" | custom-call | flops 603979776 | bytes 1179648 | tf_op jit(solution)/shard_map/pallas_call | solution.py:353
  35.5 0.1 collective-permute-start.8
  35.6 1.7 %collective-permute-done.8.other_ref = bf16[384,512]{1,0:T(8,128)(2,1)S(1)} collective-permute-done((bf16[384,512]{1,0:T(8,128)(2,1)S(1)}, bf16[384,512]{1,0:T(8,128)(2,1)S(1)}, u32[]{:S(2)}, u32[]{:S(2)}) %collective-permute-start.8) | collective-permute-done | bytes 393248 | tf_op jit(solution)/shard_map/ppermute | solution.py:365
  37.3 3.0 %shard_map.103 = bf16[1,768,1024]{2,1,0:T(8,128)(2,1)} custom-call(bf16[384,512]{1,0:T(8,128)(2,1)S(1)} %shard_map.102.mine_ref, bf16[384,512]{1,0:T(8,128)(2,1)S(1)} %collective-permute-done.8.other_ref, bf16[512,2048]{1,0:T(8,128)(2,1)S(1)} %copy-done, bf16[512,2048]{1,0:T(8,128)(2,1)S(1)} %collective-permute-done.7.w_other_ref, ...), custom_call_target="tpu_custom_call", output_to_operand_aliasing={{}: (5, {})} | custom-call | flops 1610612736 | bytes 4194304 | tf_op jit(solution)/shard_map/pallas_call | solution.py:367
Async XLA Ops:
  0.0 25.0 %collective-permute-start.7 = (bf16[512,2048]{1,0:T(8,128)(2,1)}, bf16[512,2048]{1,0:T(8,128)(2,1)S(1)}, u32[]{:S(2)}, u32[]{:S(2)}) collective-permute-start(bf16[512,2048]{1,0:T(8,128)(2,1)} %w_mine_ref.3), channel_id=1, source_target_pairs={{0,1},{1,0},{2,3},{3,2},{4,5},{5,4},{6,7},{7,6},{8,9},{9,8},{10,11... | collective-permute-start | bytes 6291464 | tf_op jit(solution)/shard_map/ppermute | solution.py:343
  0.5 9.4 %copy-start.1 = (bf16[2048,512]{1,0:T(8,128)(2,1)S(1)}, bf16[2048,512]{1,0:T(8,128)(2,1)}, u32[]{:S(2)}) copy-start(bf16[2048,512]{1,0:T(8,128)(2,1)} %weight_ref.1) | copy-start | bytes 6291460
  0.5 9.4 %copy-start.2 = (f32[2,64,128]{2,1,0:T(8,128)S(1)}, f32[2,64,128]{2,1,0:T(8,128)}, u32[]{:S(2)}) copy-start(f32[2,64,128]{2,1,0:T(8,128)} %constant.5.clone.refs_6_.fine_ref) | copy-start | bytes 196612
  0.5 9.4 %copy-start.3 = (f32[48,2,128]{2,1,0:T(2,128)S(1)}, f32[48,2,128]{2,1,0:T(2,128)}, u32[]{:S(2)}) copy-start(f32[48,2,128]{2,1,0:T(2,128)} %constant.4.clone.refs_5_.coarse_ref) | copy-start | bytes 147460
  4.6 7.4 %collective-permute-start.3 = (bf16[3,64,256]{2,1,0:T(8,128)(2,1)S(1)}, bf16[3,64,256]{2,1,0:T(8,128)(2,1)S(1)}, u32[]{:S(2)}, u32[]{:S(2)}) collective-permute-start(bf16[3,64,256]{2,1,0:T(8,128)(2,1)S(1)} %get-tuple-element.24), channel_id=1, source_target_pairs={{0,2},{2,0},{4,6},{6,4},{1,3},{3,1},{5,7},{7,5},{8,10},{10,8},{12,... | collective-permute-start | bytes 294920 | tf_op jit(solution)/shard_map/ppermute | solution.py:319
  7.3 10.8 %collective-permute-start.4 = (bf16[3,64,256]{2,1,0:T(8,128)(2,1)S(1)}, bf16[3,64,256]{2,1,0:T(8,128)(2,1)S(1)}, u32[]{:S(2)}, u32[]{:S(2)}) collective-permute-start(bf16[3,64,256]{2,1,0:T(8,128)(2,1)S(1)} %get-tuple-element.25), channel_id=1, source_target_pairs={{0,4},{2,6},{4,0},{6,2},{1,5},{3,7},{5,1},{7,3},{8,12},{10,14},{12... | collective-permute-start | bytes 294920 | tf_op jit(solution)/shard_map/ppermute | solution.py:319
  9.9 8.2 %collective-permute-start.5 = (bf16[3,64,256]{2,1,0:T(8,128)(2,1)S(1)}, bf16[3,64,256]{2,1,0:T(8,128)(2,1)S(1)}, u32[]{:S(2)}, u32[]{:S(2)}) collective-permute-start(bf16[3,64,256]{2,1,0:T(8,128)(2,1)S(1)} %get-tuple-element.26), channel_id=1, source_target_pairs={{0,6},{2,4},{4,2},{6,0},{1,7},{3,5},{5,3},{7,1},{8,14},{10,12},{12... | collective-permute-start | bytes 294920 | tf_op jit(solution)/shard_map/ppermute | solution.py:319
  12.1 12.9 %copy-start = (bf16[512,2048]{1,0:T(8,128)(2,1)S(1)}, bf16[512,2048]{1,0:T(8,128)(2,1)}, u32[]{:S(2)}) copy-start(bf16[512,2048]{1,0:T(8,128)(2,1)} %w_mine_ref.3) | copy-start | bytes 6291460
  12.1 12.9 %copy-start.4 = (f32[1024]{0:T(1024)S(1)}, f32[1024]{0:T(1024)}, u32[]{:S(2)}) copy-start(f32[1024]{0:T(1024)} %param.15) | copy-start | bytes 12292
  20.4 4.6 %collective-permute-start.6 = (bf16[384,512]{1,0:T(8,128)(2,1)S(1)}, bf16[384,512]{1,0:T(8,128)(2,1)S(1)}, u32[]{:S(2)}, u32[]{:S(2)}) collective-permute-start(bf16[384,512]{1,0:T(8,128)(2,1)S(1)} %shard_map.100.mine_ref), channel_id=1, source_target_pairs={{0,1},{1,0},{2,3},{3,2},{4,5},{5,4},{6,7},{7,6},{8,9},{9,8},{10,11... | collective-permute-start | bytes 1179656 | tf_op jit(solution)/shard_map/ppermute | solution.py:365
  20.5 7.5 %collective-permute-start = (bf16[3,64,256]{2,1,0:T(8,128)(2,1)S(1)}, bf16[3,64,256]{2,1,0:T(8,128)(2,1)S(1)}, u32[]{:S(2)}, u32[]{:S(2)}) collective-permute-start(bf16[3,64,256]{2,1,0:T(8,128)(2,1)S(1)} %get-tuple-element.20), channel_id=1, source_target_pairs={{0,2},{2,0},{4,6},{6,4},{1,3},{3,1},{5,7},{7,5},{8,10},{10,8},{12,... | collective-permute-start | bytes 294920 | tf_op jit(solution)/shard_map/ppermute | solution.py:319
  22.4 10.7 %collective-permute-start.1 = (bf16[3,64,256]{2,1,0:T(8,128)(2,1)S(1)}, bf16[3,64,256]{2,1,0:T(8,128)(2,1)S(1)}, u32[]{:S(2)}, u32[]{:S(2)}) collective-permute-start(bf16[3,64,256]{2,1,0:T(8,128)(2,1)S(1)} %get-tuple-element.21), channel_id=1, source_target_pairs={{0,4},{2,6},{4,0},{6,2},{1,5},{3,7},{5,1},{7,3},{8,12},{10,14},{12... | collective-permute-start | bytes 294920 | tf_op jit(solution)/shard_map/ppermute | solution.py:319
  23.6 9.6 %collective-permute-start.2 = (bf16[3,64,256]{2,1,0:T(8,128)(2,1)S(1)}, bf16[3,64,256]{2,1,0:T(8,128)(2,1)S(1)}, u32[]{:S(2)}, u32[]{:S(2)}) collective-permute-start(bf16[3,64,256]{2,1,0:T(8,128)(2,1)S(1)} %get-tuple-element.22), channel_id=1, source_target_pairs={{0,6},{2,4},{4,2},{6,0},{1,7},{3,5},{5,3},{7,1},{8,14},{10,12},{12... | collective-permute-start | bytes 294920 | tf_op jit(solution)/shard_map/ppermute | solution.py:319
  35.5 1.8 %collective-permute-start.8 = (bf16[384,512]{1,0:T(8,128)(2,1)S(1)}, bf16[384,512]{1,0:T(8,128)(2,1)S(1)}, u32[]{:S(2)}, u32[]{:S(2)}) collective-permute-start(bf16[384,512]{1,0:T(8,128)(2,1)S(1)} %shard_map.102.mine_ref), channel_id=1, source_target_pairs={{0,1},{1,0},{2,3},{3,2},{4,5},{5,4},{6,7},{7,6},{8,9},{9,8},{10,11... | collective-permute-start | bytes 1179656 | tf_op jit(solution)/shard_map/ppermute | solution.py:365

commit v3 on v2

--- a/solution.py
+++ b/solution.py
@@ -17,7 +17,7 @@
 NORM_EPS = 1e-06
 LOG2E = 1.4426950408889634
 GROUPS = (3, 3)
-PER_DOT = 2
+PER_DOT = 4
 OUT_SPLIT = 2
 
 
@@ -63,10 +63,10 @@
 
 
 def kv_kernel(plan, chunk, *refs):
-    owner_hbm, part_hbm, tokens_ref, wk_ref, wv_ref, coarse_hbm, fine_hbm = refs[:7]
-    kv_ref, bias_ref, tok = refs[7:10]
-    send_refs = refs[10 : 10 + len(plan)]
-    weight, coarse_ref, fine_ref, owner_ref, part_ref, tok_sem, sem = refs[10 + len(plan) :]
+    owner_hbm, part_hbm, tokens_ref, wk_ref, wv_ref, coarse_hbm, fine_hbm, wq_hbm, wo_hbm = refs[:9]
+    kv_ref, bias_ref, tok, coarse_ref, fine_ref, wq_ref, wo_ref = refs[9:16]
+    send_refs = refs[16 : 16 + len(plan)]
+    weight, owner_ref, part_ref, tok_sem, sem = refs[16 + len(plan) :]
     rows = tok.shape[0]
     me = lax.axis_index("kv")
     per_chunk = chunk // KEY_BLOCK
@@ -79,6 +79,8 @@
         (fine_hbm, fine_ref),
         (owner_hbm, owner_ref),
         (part_hbm, part_ref),
+        (wq_hbm, wq_ref),
+        (wo_hbm, wo_ref),
     ]
     small = [pltpu.make_async_copy(src, dst, sem.at[at]) for at, (src, dst) in enumerate(small)]
     t_copies = [
@@ -87,7 +89,8 @@
         )
         for at in range(rows // chunk)
     ]
-    for copy in small[:2] + t_copies[:1] + small[2:] + t_copies[1:]:
+    small, later = small[:-2], small[-2:]
+    for copy in small[:2] + t_copies[:1] + small[2:] + t_copies[1:] + later:
         copy.start()
     for copy in small:
         copy.wait()
@@ -127,12 +130,12 @@
                 [jnp.logical_and(source_id == at, owner >= 0) for at, owner in enumerate(owners)],
             )
         bias_ref[row] = jnp.where(named, jnp.float32(0), jnp.float32(-jnp.inf))
+    for copy in later:
+        copy.wait()
 
 
 def q_kernel(chunk, tok_ref, weight_ref, coarse_ref, fine_ref, out_ref):
     rows, tiles = tok_ref.shape[0], weight_ref.shape[1] // LANES
-    blocks = rows // KEY_BLOCK
-    me = lax.axis_index("kv")
     low = lax.broadcasted_iota(jnp.int32, (KEY_BLOCK, LANES), 1) < HEAD_DIM
     per_chunk = chunk // KEY_BLOCK
     for at in range(rows // chunk):
@@ -141,7 +144,7 @@
         ) * (HEAD_DIM ** -0.5)
         for sub in range(per_chunk):
             block = at * per_chunk + sub
-            cosine, sine = block_angles(coarse_ref, fine_ref, me * blocks + block)
+            cosine, sine = block_angles(coarse_ref, fine_ref, block)
             span = slice(block * KEY_BLOCK, (block + 1) * KEY_BLOCK)
             for tile in range(tiles):
                 piece = rotate_tile(
@@ -158,7 +161,8 @@
                 out_ref[2 * tile + 1, span] = odd.astype(BF16)
 
 
-def attention_kernel(first, sources, per_dot, q_ref, own_ref, bias_ref, *refs):
+def attention_kernel(first, offsets, per_dot, q_ref, own_ref, bias_ref, *refs):
+    sources = len(offsets)
     source_refs, out_ref = refs[:sources], refs[-1]
     heads = q_ref.shape[0]
     pairs = heads // 2
@@ -170,7 +174,7 @@
     per_query = QUERY_BLOCK // KEY_BLOCK
     for row in range(out_ref.shape[0] // QUERY_BLOCK):
         block = first + row
-        picks = [ref[row] for ref in source_refs]
+        picks = [ref[offset + row] for ref, offset in zip(source_refs, offsets)]
         picks += [own_ref[block * per_query + at] for at in range(per_query)]
         keys = jnp.concatenate([p[:, :LANES] for p in picks], axis=0)
         values = jnp.concatenate([p[:, LANES:] for p in picks], axis=0)
@@ -202,29 +206,47 @@
                 ] = (top / bottom).astype(BF16)
 
 
-def out_kernel(first, split, mine_ref, other_ref, w_mine_ref, w_other_ref, gain_ref, *refs):
+def column_start(half, me, cols, at, width):
+    return pl.multiple_of((me if half == 0 else 1 - me) * cols + at * width, width)
+
+
+def weight_columns(ref, start, width):
+    heads = ref.shape[0] // HEAD_DIM
+    order = [h for p in range(heads // 2) for h in (p, p + heads // 2)]
+    return jnp.concatenate(
+        [ref[h * HEAD_DIM : (h + 1) * HEAD_DIM, pl.ds(start, width)] for h in order], axis=0
+    )
+
+
+def partial_kernel(mine_ref, weight_ref, out_ref):
+    width = 256
+    mine = mine_ref[...]
+    for at in range(out_ref.shape[1] // width):
+        span = slice(at * width, (at + 1) * width)
+        out_ref[:, span] = jnp.dot(
+            mine, weight_columns(weight_ref, at * width, width), preferred_element_type=F32
+        ).astype(BF16)
+
+
+def out_kernel(first, split, partial_ref, other_ref, weight_ref, gain_ref, *refs):
     out_hbm, kept, staged, sem = refs[-4:]
     rows, cols = staged.shape
-    depth = w_mine_ref.shape[0]
-    heads = depth // HEAD_DIM
     me = lax.axis_index("tp")
     width = 256
-    order = [h for p in range(heads // 2) for h in (p, p + heads // 2)]
     tile = rows // split
     copies = []
     for part in range(split):
         span = slice(part * tile, (part + 1) * tile)
-        mine, other = mine_ref[span], other_ref[span]
+        other = other_ref[span]
         total = None
         for half in range(2):
             for at in range(cols // width):
-                start = pl.multiple_of((me if half == 0 else 1 - me) * cols + at * width, width)
-                load = lambda ref: jnp.concatenate(
-                    [ref[h * HEAD_DIM : (h + 1) * HEAD_DIM, pl.ds(start, width)] for h in order], axis=0
+                start = column_start(half, me, cols, at, width)
+                theirs = jnp.dot(
+                    other, weight_columns(weight_ref, start, width), preferred_element_type=F32
                 )
-                a = jnp.dot(mine, load(w_mine_ref), preferred_element_type=F32)
-                b = jnp.dot(other, load(w_other_ref), preferred_element_type=F32)
-                projected = a.astype(BF16).astype(F32) + b.astype(BF16).astype(F32)
+                mine = partial_ref[span, pl.ds(start, width)].astype(F32)
+                projected = mine + theirs.astype(BF16).astype(F32)
                 if half == 0:
                     kept[span, at * width : (at + 1) * width] = projected
                 squares = projected * projected
@@ -270,55 +292,66 @@
     sizes = GROUPS if direct and sum(GROUPS) == qblocks else (qblocks,)
     firsts = [sum(sizes[:g]) for g in range(len(sizes))]
     sources = devices if direct else chosen
-    plan = (
-        [("pair", pair, firsts[g]) for g in range(len(sizes)) for pair in range(devices)]
-        if direct
-        else [("all", 0, 0)]
-    )
+    whole = (0, 1) if len(sizes) > 1 else ()
+    pieces = [(pair, None) for pair in whole]
+    pieces += [(pair, g) for g in range(len(sizes)) for pair in range(devices) if pair not in whole]
+    extent = lambda g: (0, qblocks) if g is None else (firsts[g], sizes[g])
+    plan = [("pair", pair, extent(g)[0]) for pair, g in pieces] if direct else [("all", 0, 0)]
     block_shape = (KEY_BLOCK, 2 * LANES)
     sends = (
-        [pltpu.VMEM((sizes[g],) + block_shape, BF16) for g in range(len(sizes)) for _ in range(devices)]
+        [pltpu.VMEM((extent(g)[1],) + block_shape, BF16) for _, g in pieces]
         if direct
         else [jax.ShapeDtypeStruct((devices * qblocks,) + block_shape, BF16)]
     )
     chunk = 256
-    table_scratch = [pltpu.VMEM((per_device, 2, LANES), F32), pltpu.VMEM((2, KEY_BLOCK, LANES), F32)]
     kv_out = pl.pallas_call(
         functools.partial(kv_kernel, plan, chunk),
         out_shape=[
             pltpu.VMEM((per_device,) + block_shape, BF16),
             pltpu.VMEM((qblocks, 1, sources * KEY_BLOCK), F32),
             pltpu.VMEM((tok_count, width), BF16),
+            pltpu.VMEM((per_device, 2, LANES), F32),
+            pltpu.VMEM((2, KEY_BLOCK, LANES), F32),
+            pltpu.VMEM(query_weight.shape, BF16),
+            pltpu.VMEM(out_weight.shape, BF16),
         ]
         + sends,
-        in_specs=[hb] * 7,
-        out_specs=[vm] * (3 + len(sends)),
+        in_specs=[hb] * 9,
+        out_specs=[vm] * (7 + len(sends)),
         scratch_shapes=[
             pltpu.VMEM((width, 2 * LANES), BF16),
-            *table_scratch,
             pltpu.SMEM(owner_t.shape, jnp.int32),
             pltpu.SMEM(part_t.shape, jnp.int32),
             pltpu.SemaphoreType.DMA((tok_count // chunk,)),
-            pltpu.SemaphoreType.DMA((6,)),
+            pltpu.SemaphoreType.DMA((8,)),
         ],
         compiler_params=pltpu.CompilerParams(vmem_limit_bytes=24 << 20),
         name="kv_project",
         cost_estimate=pl.CostEstimate(
             flops=2 * tok_count * width * 2 * LANES, bytes_accessed=4 * tok_count * width, transcendentals=0
         ),
-    )(*map(distant, (owner_t, part_t, tokens, key_weight, value_weight, coarse, fine)))
-    kv_rows, bias, loaded, sent = kv_out[0], kv_out[1], kv_out[2], list(kv_out[3:])
+    )(
+        *map(
+            distant,
+            (owner_t, part_t, tokens, key_weight, value_weight, coarse, fine, query_weight, out_weight),
+        )
+    )
+    kv_rows, bias, *loaded, my_weight = kv_out[:7]
+    sent = list(kv_out[7:])
 
     if direct:
-        by_group = []
-        for g in range(len(sizes)):
-            arrived = []
-            for pair in range(devices):
-                block = sent[g * devices + pair]
-                if pair:
-                    block = lax.ppermute(block, "kv", [(i, i ^ pair) for i in range(devices)])
-                arrived.append(resident(block))
-            by_group.append(arrived)
+        arrived = {}
+        for (pair, g), block in zip(pieces, sent):
+            if pair:
+                block = lax.ppermute(block, "kv", [(i, i ^ pair) for i in range(devices)])
+            arrived[pair, g] = resident(block)
+        by_group = [
+            [arrived[pair, None if pair in whole else g] for pair in range(devices)]
+            for g in range(len(sizes))
+        ]
+        offsets = [
+            [firsts[g] if pair in whole else 0 for pair in range(devices)] for g in range(len(sizes))
+        ]
     else:
         got = lax.all_to_all(
             sent[0].reshape((devices, qblocks) + block_shape), "kv", split_axis=0, concat_axis=0, tiled=True
@@ -326,6 +359,7 @@
         mine_owner = lax.dynamic_slice_in_dim(owner_t, me * qblocks, qblocks, 1)
         rows = jnp.arange(qblocks, dtype=jnp.int32)
         by_group = [[got[jnp.maximum(mine_owner[slot], 0), rows] for slot in range(chosen)]]
+        offsets = [[0] * chosen]
 
     queries = pl.pallas_call(
         functools.partial(q_kernel, chunk),
@@ -339,9 +373,9 @@
             bytes_accessed=4 * tok_count * width,
             transcendentals=0,
         ),
-    )(*map(resident, (loaded, query_weight, coarse, fine)))
-    other_weight = resident(lax.ppermute(out_weight, "tp", swap))
-    my_weight = resident(out_weight)
+    )(*map(resident, (loaded[0], loaded[3], loaded[1], loaded[2])))
+    other_weight = resident(lax.ppermute(my_weight, "tp", swap))
+    my_weight = resident(my_weight)
 
     gain = norm_gain.reshape(1, -1)
     cols = norm_gain.shape[0]
@@ -351,7 +385,7 @@
         tokens_here = size * QUERY_BLOCK
         extra = [] if result is None else [result]
         mixed = pl.pallas_call(
-            functools.partial(attention_kernel, first, sources, PER_DOT),
+            functools.partial(attention_kernel, first, tuple(offsets[g]), PER_DOT),
             out_shape=pltpu.VMEM((tokens_here, depth), BF16),
             in_specs=[vm] * (3 + sources) + [hb] * len(extra),
             out_specs=vm,
@@ -363,25 +397,32 @@
             ),
         )(resident(queries), resident(kv_rows), resident(bias), *by_group[g], *map(distant, extra))
         other_mixed = resident(lax.ppermute(mixed, "tp", swap))
-        split = OUT_SPLIT
+        own_partial = pl.pallas_call(
+            partial_kernel,
+            out_shape=pltpu.VMEM((tokens_here, 2 * cols), BF16),
+            in_specs=[vm] * 2,
+            out_specs=vm,
+            compiler_params=pltpu.CompilerParams(vmem_limit_bytes=16 << 20),
+            cost_estimate=pl.CostEstimate(
+                flops=4 * tokens_here * depth * cols, bytes_accessed=4 * depth * cols, transcendentals=0
+            ),
+        )(resident(mixed), my_weight)
         result = pl.pallas_call(
-            functools.partial(out_kernel, first, split),
+            functools.partial(out_kernel, first, OUT_SPLIT),
             out_shape=jax.ShapeDtypeStruct((1, tok_count, cols), BF16),
-            in_specs=[vm, vm, vm, vm, vm] + [hb] * len(extra),
+            in_specs=[vm, vm, vm, vm] + [hb] * len(extra),
             out_specs=hb,
-            input_output_aliases={5: 0} if extra else {},
+            input_output_aliases={4: 0} if extra else {},
             scratch_shapes=[
                 pltpu.VMEM((tokens_here, cols), F32),
                 pltpu.VMEM((tokens_here, cols), BF16),
-                pltpu.SemaphoreType.DMA((split,)),
+                pltpu.SemaphoreType.DMA((OUT_SPLIT,)),
             ],
-            compiler_params=pltpu.CompilerParams(vmem_limit_bytes=24 << 20),
+            compiler_params=pltpu.CompilerParams(vmem_limit_bytes=16 << 20),
             cost_estimate=pl.CostEstimate(
-                flops=8 * tokens_here * depth * cols,
-                bytes_accessed=8 * depth * cols,
-                transcendentals=0,
+                flops=4 * tokens_here * depth * cols, bytes_accessed=4 * depth * cols, transcendentals=0
             ),
-        )(resident(mixed), other_mixed, my_weight, other_weight, gain, *map(distant, extra))
+        )(resident(own_partial), other_mixed, other_weight, gain, *map(distant, extra))
     return result
 
 

time: 40.4 us -> 38.4 us (0.950)
  starting transfers between devices: 10.4 us -> 9.04 us
  waiting for transfers between devices: 12.9 us -> 11.9 us
    ppermute x6 -> x5, starting transfers between devices: 9.73 us -> 8.34 us  [body(): block = lax.ppermute(block, 'kv', [(i, i ^ pair) for i in range(devices)])]
    ppermute x2, waiting for transfers between devices: 1.71 us -> 0.71 us  [body(): other_mixed = resident(lax.ppermute(mixed, 'tp', swap))]
    pallas_call x4 -> x6, Pallas kernels: 10.6 us -> 10.9 us  [the longest x2 4.62 us: body(): pl.pallas_call(functools.partial(out_kernel, first, OUT_SPLIT), out_shape...]
    ppermute x6 -> x5, waiting for transfers between devices: 11.2 us -> 11.2 us  [body(): block = lax.ppermute(block, 'kv', [(i, i ^ pair) for i in range(devices)])]
  transfers between devices with their start and end apart: 9 -> 8, of which waited for: 3 -> 4; matrix products, arithmetic and copies ran while one was open for 0% -> 0% of each run, Pallas kernels for 29% -> 23%
where the time goes in v3:
time: 38.4 us; the launch traced here: 38.2 us
  Pallas kernels  17.2 us (45%)
  waiting for transfers between devices  11.9 us (31%)
  starting transfers between devices  9.04 us (24%)
    ppermute x5, waiting for transfers between devices, body(): block = lax.ppermute(block, 'kv', [(i, i ^ pair) for i in range(devices)])  11.2 us
    ppermute x5, starting transfers between devices, body(): block = lax.ppermute(block, 'kv', [(i, i ^ pair) for i in range(devices)])  8.34 us
    pallas_call x2, Pallas kernels, body(): pl.pallas_call(functools.partial(out_kernel, first, OUT_SPLIT), out_shape...  4.62 us
    pallas_call x2, Pallas kernels, body(): pl.pallas_call(functools.partial(attention_kernel, first, tuple(offsets[g...  4.27 us
    pallas_call x1, Pallas kernels, body(): pl.pallas_call(functools.partial(kv_kernel, plan, chunk), out_shape=[pltp...  4.03 us
    pallas_call x1, Pallas kernels, body(): pl.pallas_call(functools.partial(q_kernel, chunk), out_shape=pltpu.VMEM((...  2.26 us
    pallas_call x2, Pallas kernels, body(): pl.pallas_call(partial_kernel, out_shape=pltpu.VMEM((tokens_here, 2 * col...  1.98 us
  transfers between devices with their start and end apart: 8, of which 4 were waited for; matrix products, arithmetic and copies ran while one was open for 0% of the time, Pallas kernels for 23%

profile of v3, /device:TPU:0, one launch (start us, length us, event | category | flops | bytes accessed | tf_op | source)
XLA Modules:
  0.0 38.2 jit_solution(590637565474916964)
XLA Ops:
  0.0 4.0 %kv_project.1 = (bf16[12,64,256]{2,1,0:T(8,128)(2,1)S(1)}, f32[6,1,256]{2,1,0:T(1,128)S(1)}, bf16[768,2048]{1,0:T(8,128)(2,1)S(1)}, f32[12,2,128]{2,1,0:T(2,128)...) custom-call(s32[4,24]{1,0:T(4,128)} %bitcast.9, ...), custom_call_target="tpu_custom_call" | custom-call | flops 805306368 | bytes 6291456 | tf_op jit(solution)/shard_map/kv_project/pallas_call | solution.py:307
  4.0 0.6 %collective-permute-start.6 = (bf16[512,2048]{1,0:T(8,128)(2,1)S(1)}, bf16[512,2048]{1,0:T(8,128)(2,1)S(1)}, u32[]{:S(2)}, u32[]{:S(2)}) collective-permute-start(bf16[512,2048]{1,0:T(8,128)(2,1)S(1)} %get-tuple-element.30.weight_ref), channel_id=1, source_target_pairs={{0,1},{1,0},{2,3},{3,2},{4,5},{5,4},{6,7},{7,6},{8,9},{9,8},{10,11... | collective-permute-start | bytes 6291464 | tf_op jit(solution)/shard_map/ppermute | solution.py:377
  4.6 2.6 %collective-permute-start = (bf16[6,64,256]{2,1,0:T(8,128)(2,1)S(1)}, bf16[6,64,256]{2,1,0:T(8,128)(2,1)S(1)}, u32[]{:S(2)}, u32[]{:S(2)}) collective-permute-start(bf16[6,64,256]{2,1,0:T(8,128)(2,1)S(1)} %get-tuple-element.25), channel_id=1, source_target_pairs={{0,2},{2,0},{4,6},{6,4},{1,3},{3,1},{5,7},{7,5},{8,10},{10,8},{12,... | collective-permute-start | bytes 589832 | tf_op jit(solution)/shard_map/ppermute | solution.py:346
  7.2 2.6 %collective-permute-start.3 = (bf16[3,64,256]{2,1,0:T(8,128)(2,1)S(1)}, bf16[3,64,256]{2,1,0:T(8,128)(2,1)S(1)}, u32[]{:S(2)}, u32[]{:S(2)}) collective-permute-start(bf16[3,64,256]{2,1,0:T(8,128)(2,1)S(1)} %get-tuple-element.28), channel_id=1, source_target_pairs={{0,4},{2,6},{4,0},{6,2},{1,5},{3,7},{5,1},{7,3},{8,12},{10,14},{12... | collective-permute-start | bytes 294920 | tf_op jit(solution)/shard_map/ppermute | solution.py:346
  9.8 0.0 collective-permute-start.4
  9.8 2.3 %q_project.1.q_ref = bf16[8,768,128]{2,1,0:T(8,128)(2,1)S(1)} custom-call(bf16[768,2048]{1,0:T(8,128)(2,1)S(1)} %get-tuple-element.18.tok_ref, bf16[2048,512]{1,0:T(8,128)(2,1)S(1)} %get-tuple-element.19.weight_ref, f32[12,2,128]{2,1,0:T(2,128)S(1)} %get-tuple-element.20.coarse_ref, f32[2,64,128]{2,1,0:T(8,128)S(1)} %get-tuple-element.21.fine_ref), custom_call_target="tpu_custom_call" | custom-call | flops 1610612736 | bytes 6291456 | tf_op jit(solution)/shard_map/q_project/pallas_call | solution.py:364
  12.1 2.6 %collective-permute-done.3.refs_2_ = bf16[3,64,256]{2,1,0:T(8,128)(2,1)S(1)} collective-permute-done((bf16[3,64,256]{2,1,0:T(8,128)(2,1)S(1)}, bf16[3,64,256]{2,1,0:T(8,128)(2,1)S(1)}, u32[]{:S(2)}, u32[]{:S(2)}) %collective-permute-start.3) | collective-permute-done | bytes 98336 | tf_op jit(solution)/shard_map/ppermute | solution.py:346
  14.7 4.6 %collective-permute-done.4.refs_3_ = bf16[3,64,256]{2,1,0:T(8,128)(2,1)S(1)} collective-permute-done((bf16[3,64,256]{2,1,0:T(8,128)(2,1)S(1)}, bf16[3,64,256]{2,1,0:T(8,128)(2,1)S(1)}, u32[]{:S(2)}, u32[]{:S(2)}) %collective-permute-start.4) | collective-permute-done | bytes 98336 | tf_op jit(solution)/shard_map/ppermute | solution.py:346
  19.2 0.0 collective-permute-done.refs_1_
  19.2 2.1 %shard_map.100.mine_ref = bf16[384,512]{1,0:T(8,128)(2,1)S(1)} custom-call(bf16[8,768,128]{2,1,0:T(8,128)(2,1)S(1)} %q_project.1.q_ref, bf16[12,64,256]{2,1,0:T(8,128)(2,1)S(1)} %get-tuple-element.22.own_ref, f32[6,1,256]{2,1,0:T(1,128)S(1)} %get-tuple-element.23.bias_ref, bf16[6,64,256]{2,1,0:T(8,128)(2,1)S(1)} %get-tuple-element.24.refs_0_, ...), custom_call_target="tpu_custom_call" | custom-call | flops 603979776 | bytes 1179648 | tf_op jit(solution)/shard_map/pallas_call | solution.py:387
  21.4 0.0 copy-start
  21.4 0.1 collective-permute-start.5
  21.5 1.8 %collective-permute-start.1 = (bf16[3,64,256]{2,1,0:T(8,128)(2,1)S(1)}, bf16[3,64,256]{2,1,0:T(8,128)(2,1)S(1)}, u32[]{:S(2)}, u32[]{:S(2)}) collective-permute-start(bf16[3,64,256]{2,1,0:T(8,128)(2,1)S(1)} %get-tuple-element.26), channel_id=1, source_target_pairs={{0,4},{2,6},{4,0},{6,2},{1,5},{3,7},{5,1},{7,3},{8,12},{10,14},{12... | collective-permute-start | bytes 294920 | tf_op jit(solution)/shard_map/ppermute | solution.py:346
  23.2 1.3 %collective-permute-start.2 = (bf16[3,64,256]{2,1,0:T(8,128)(2,1)S(1)}, bf16[3,64,256]{2,1,0:T(8,128)(2,1)S(1)}, u32[]{:S(2)}, u32[]{:S(2)}) collective-permute-start(bf16[3,64,256]{2,1,0:T(8,128)(2,1)S(1)} %get-tuple-element.27), channel_id=1, source_target_pairs={{0,6},{2,4},{4,2},{6,0},{1,7},{3,5},{5,3},{7,1},{8,14},{10,12},{12... | collective-permute-start | bytes 294920 | tf_op jit(solution)/shard_map/ppermute | solution.py:346
  24.6 1.0 %shard_map.101.partial_ref = bf16[384,2048]{1,0:T(8,128)(2,1)S(1)} custom-call(bf16[384,512]{1,0:T(8,128)(2,1)S(1)} %shard_map.100.mine_ref, bf16[512,2048]{1,0:T(8,128)(2,1)S(1)} %get-tuple-element.30.weight_ref), custom_call_target="tpu_custom_call" | custom-call | flops 805306368 | bytes 2097152 | tf_op jit(solution)/shard_map/pallas_call | solution.py:400
  25.6 0.0 collective-permute-done.5.other_ref
  25.6 0.0 collective-permute-done.6.weight_ref
  25.6 0.0 copy-done
  25.6 2.3 %shard_map.102.refs_4_.refs_0_ = bf16[1,768,1024]{2,1,0:T(8,128)(2,1)} custom-call(bf16[384,2048]{1,0:T(8,128)(2,1)S(1)} %shard_map.101.partial_ref, bf16[384,512]{1,0:T(8,128)(2,1)S(1)} %collective-permute-done.5.other_ref, bf16[512,2048]{1,0:T(8,128)(2,1)S(1)} %collective-permute-done.6.weight_ref, f32[1,1024]{1,0:T(1,128)S(1)} %bitcast.7), custom_call_target="tpu_custom_call" | custom-call | flops 805306368 | bytes 2097152 | tf_op jit(solution)/shard_map/pallas_call | solution.py:410
  27.9 4.1 %collective-permute-done.1.refs_2_ = bf16[3,64,256]{2,1,0:T(8,128)(2,1)S(1)} collective-permute-done((bf16[3,64,256]{2,1,0:T(8,128)(2,1)S(1)}, bf16[3,64,256]{2,1,0:T(8,128)(2,1)S(1)}, u32[]{:S(2)}, u32[]{:S(2)}) %collective-permute-start.1) | collective-permute-done | bytes 98336 | tf_op jit(solution)/shard_map/ppermute | solution.py:346
  32.0 0.0 collective-permute-done.2.refs_3_
  32.0 2.1 %shard_map.103.mine_ref = bf16[384,512]{1,0:T(8,128)(2,1)S(1)} custom-call(bf16[8,768,128]{2,1,0:T(8,128)(2,1)S(1)} %q_project.1.q_ref, bf16[12,64,256]{2,1,0:T(8,128)(2,1)S(1)} %get-tuple-element.22.own_ref, f32[6,1,256]{2,1,0:T(1,128)S(1)} %get-tuple-element.23.bias_ref, bf16[6,64,256]{2,1,0:T(8,128)(2,1)S(1)} %get-tuple-element.24.refs_0_, ...), custom_call_target="tpu_custom_call" | custom-call | flops 603979776 | bytes 1179648 | tf_op jit(solution)/shard_map/pallas_call | solution.py:387
  34.1 0.1 collective-permute-start.7
  34.2 1.0 %shard_map.104.partial_ref = bf16[384,2048]{1,0:T(8,128)(2,1)S(1)} custom-call(bf16[384,512]{1,0:T(8,128)(2,1)S(1)} %shard_map.103.mine_ref, bf16[512,2048]{1,0:T(8,128)(2,1)S(1)} %get-tuple-element.30.weight_ref), custom_call_target="tpu_custom_call" | custom-call | flops 805306368 | bytes 2097152 | tf_op jit(solution)/shard_map/pallas_call | solution.py:400
  35.2 0.7 %collective-permute-done.7.other_ref = bf16[384,512]{1,0:T(8,128)(2,1)S(1)} collective-permute-done((bf16[384,512]{1,0:T(8,128)(2,1)S(1)}, bf16[384,512]{1,0:T(8,128)(2,1)S(1)}, u32[]{:S(2)}, u32[]{:S(2)}) %collective-permute-start.7) | collective-permute-done | bytes 393248 | tf_op jit(solution)/shard_map/ppermute | solution.py:399
  35.9 2.3 %shard_map.105 = bf16[1,768,1024]{2,1,0:T(8,128)(2,1)} custom-call(bf16[384,2048]{1,0:T(8,128)(2,1)S(1)} %shard_map.104.partial_ref, bf16[384,512]{1,0:T(8,128)(2,1)S(1)} %collective-permute-done.7.other_ref, bf16[512,2048]{1,0:T(8,128)(2,1)S(1)} %collective-permute-done.6.weight_ref, f32[1,1024]{1,0:T(1,128)S(1)} %bitcast.8, ...), custom_call_target="tpu_custom_call", output_to_operand_aliasing={{}: (4, {})} | custom-call | flops 805306368 | bytes 2097152 | tf_op jit(solution)/shard_map/pallas_call | solution.py:410
Async XLA Ops:
  4.0 21.6 %collective-permute-start.6 = (bf16[512,2048]{1,0:T(8,128)(2,1)S(1)}, bf16[512,2048]{1,0:T(8,128)(2,1)S(1)}, u32[]{:S(2)}, u32[]{:S(2)}) collective-permute-start(bf16[512,2048]{1,0:T(8,128)(2,1)S(1)} %get-tuple-element.30.weight_ref), channel_id=1, source_target_pairs={{0,1},{1,0},{2,3},{3,2},{4,5},{5,4},{6,7},{7,6},{8,9},{9,8},{10,11... | collective-permute-start | bytes 6291464 | tf_op jit(solution)/shard_map/ppermute | solution.py:377
  4.6 14.6 %collective-permute-start = (bf16[6,64,256]{2,1,0:T(8,128)(2,1)S(1)}, bf16[6,64,256]{2,1,0:T(8,128)(2,1)S(1)}, u32[]{:S(2)}, u32[]{:S(2)}) collective-permute-start(bf16[6,64,256]{2,1,0:T(8,128)(2,1)S(1)} %get-tuple-element.25), channel_id=1, source_target_pairs={{0,2},{2,0},{4,6},{6,4},{1,3},{3,1},{5,7},{7,5},{8,10},{10,8},{12,... | collective-permute-start | bytes 589832 | tf_op jit(solution)/shard_map/ppermute | solution.py:346
  7.2 7.4 %collective-permute-start.3 = (bf16[3,64,256]{2,1,0:T(8,128)(2,1)S(1)}, bf16[3,64,256]{2,1,0:T(8,128)(2,1)S(1)}, u32[]{:S(2)}, u32[]{:S(2)}) collective-permute-start(bf16[3,64,256]{2,1,0:T(8,128)(2,1)S(1)} %get-tuple-element.28), channel_id=1, source_target_pairs={{0,4},{2,6},{4,0},{6,2},{1,5},{3,7},{5,1},{7,3},{8,12},{10,14},{12... | collective-permute-start | bytes 294920 | tf_op jit(solution)/shard_map/ppermute | solution.py:346
  9.8 9.4 %collective-permute-start.4 = (bf16[3,64,256]{2,1,0:T(8,128)(2,1)S(1)}, bf16[3,64,256]{2,1,0:T(8,128)(2,1)S(1)}, u32[]{:S(2)}, u32[]{:S(2)}) collective-permute-start(bf16[3,64,256]{2,1,0:T(8,128)(2,1)S(1)} %get-tuple-element.29), channel_id=1, source_target_pairs={{0,6},{2,4},{4,2},{6,0},{1,7},{3,5},{5,3},{7,1},{8,14},{10,12},{12... | collective-permute-start | bytes 294920 | tf_op jit(solution)/shard_map/ppermute | solution.py:346
  21.4 4.2 %copy-start = (f32[1024]{0:T(1024)S(1)}, f32[1024]{0:T(1024)}, u32[]{:S(2)}) copy-start(f32[1024]{0:T(1024)} %param.15) | copy-start | bytes 12292
  21.4 4.2 %collective-permute-start.5 = (bf16[384,512]{1,0:T(8,128)(2,1)S(1)}, bf16[384,512]{1,0:T(8,128)(2,1)S(1)}, u32[]{:S(2)}, u32[]{:S(2)}) collective-permute-start(bf16[384,512]{1,0:T(8,128)(2,1)S(1)} %shard_map.100.mine_ref), channel_id=1, source_target_pairs={{0,1},{1,0},{2,3},{3,2},{4,5},{5,4},{6,7},{7,6},{8,9},{9,8},{10,11... | collective-permute-start | bytes 1179656 | tf_op jit(solution)/shard_map/ppermute | solution.py:399
  21.5 10.5 %collective-permute-start.1 = (bf16[3,64,256]{2,1,0:T(8,128)(2,1)S(1)}, bf16[3,64,256]{2,1,0:T(8,128)(2,1)S(1)}, u32[]{:S(2)}, u32[]{:S(2)}) collective-permute-start(bf16[3,64,256]{2,1,0:T(8,128)(2,1)S(1)} %get-tuple-element.26), channel_id=1, source_target_pairs={{0,4},{2,6},{4,0},{6,2},{1,5},{3,7},{5,1},{7,3},{8,12},{10,14},{12... | collective-permute-start | bytes 294920 | tf_op jit(solution)/shard_map/ppermute | solution.py:346
  23.2 8.8 %collective-permute-start.2 = (bf16[3,64,256]{2,1,0:T(8,128)(2,1)S(1)}, bf16[3,64,256]{2,1,0:T(8,128)(2,1)S(1)}, u32[]{:S(2)}, u32[]{:S(2)}) collective-permute-start(bf16[3,64,256]{2,1,0:T(8,128)(2,1)S(1)} %get-tuple-element.27), channel_id=1, source_target_pairs={{0,6},{2,4},{4,2},{6,0},{1,7},{3,5},{5,3},{7,1},{8,14},{10,12},{12... | collective-permute-start | bytes 294920 | tf_op jit(solution)/shard_map/ppermute | solution.py:346
  34.1 1.8 %collective-permute-start.7 = (bf16[384,512]{1,0:T(8,128)(2,1)S(1)}, bf16[384,512]{1,0:T(8,128)(2,1)S(1)}, u32[]{:S(2)}, u32[]{:S(2)}) collective-permute-start(bf16[384,512]{1,0:T(8,128)(2,1)S(1)} %shard_map.103.mine_ref), channel_id=1, source_target_pairs={{0,1},{1,0},{2,3},{3,2},{4,5},{5,4},{6,7},{7,6},{8,9},{9,8},{10,11... | collective-permute-start | bytes 1179656 | tf_op jit(solution)/shard_map/ppermute | solution.py:399
